TPU v7x, 32 devices: a whole 2x2x4 slice. The times are simulated.
32 devices in a mesh: dp: 4 (over y, x), kv: 4 (over z), tp: 2 (over core).
Axes of the slice: x: 2, y: 2, z: 4, core: 2. Of those that a mesh axis runs over, the one named last changes fastest.
Arguments:
- tokens: bfloat16 [16, 4096], P('dp', ('kv', 'tp')), parts along dimension 0, may hold values from -6 to 6
- mix_gain: float32 [4096], replicated, may hold values from 0.1 to 1.9
- w_query: bfloat16 [4096, 2048], P('kv', 'tp'), may hold values from -0.09375 to 0.09375
- w_key: bfloat16 [4096, 2048], P('kv', 'tp'), may hold values from -0.09375 to 0.09375
- w_value: bfloat16 [4096, 4096], P('kv', 'tp'), may hold values from -0.09375 to 0.09375
- w_igate: bfloat16 [4096, 16], replicated, may hold values from -0.09375 to 0.09375
- w_fgate: bfloat16 [4096, 16], replicated, may hold values from -0.09375 to 0.09375
- igate_bias: float32 [16], replicated, may hold values from -3 to 1
- fgate_bias: float32 [16], replicated, may hold values from -2 to 5
- memory: float32 [16, 16, 256, 128], P(('dp', 'kv'), 'tp'), parts along dimension 0, may hold values from -6 to 6
- normalizer: float32 [16, 16, 128], P(('dp', 'kv'), 'tp'), parts along dimension 0, may hold values from -6 to 6
- stabilizer: float32 [16, 16], P(('dp', 'kv'), 'tp'), parts along dimension 0, may hold values from -3 to 3
- w_output: bfloat16 [4096, 4096], P('tp', 'kv'), may hold values from -0.09375 to 0.09375
- mlp_gain: float32 [4096], replicated, may hold values from 0.1 to 1.9
- w_up: bfloat16 [4096, 16384], P(None, ('kv', 'tp')), may hold values from -0.09375 to 0.09375
- w_down: bfloat16 [16384, 4096], P(('kv', 'tp')), may hold values from -0.0625 to 0.0625
Outputs:
- new_tokens: bfloat16 [16, 4096], P('dp', ('kv', 'tp')), parts along dimension 0
- new_memory: float32 [16, 16, 256, 128], P(('dp', 'kv'), 'tp'), parts along dimension 0
- new_normalizer: float32 [16, 16, 128], P(('dp', 'kv'), 'tp'), parts along dimension 0
- new_stabilizer: float32 [16, 16], P(('dp', 'kv'), 'tp'), parts along dimension 0
There are 4 independent parts, one for each index of `dp`. A program takes and returns all parts, laid end to end along the dimension named above; an argument that names none is the same for every part. Nothing has to cross between parts.
All inputs are finite; a program needn't handle non-finite values.
Results may differ from a plain program's by a relative error of at most 0.019.
Values may be sent and summed in bfloat16 or wider, within the bound.
A program may use at most 128 MiB of HBM per device.

v0:
```python
import functools

import jax
import jax.numpy as jnp
from jax import lax
from jax.experimental import pallas as pl
from jax.experimental.pallas import tpu as pltpu
from jax.sharding import PartitionSpec as P

MESH = pl.DeviceIdType.MESH
F32 = jnp.float32
BF16 = jnp.bfloat16
LANES = 128


norm_eps = 1e-06


def rms_normed(rows, gain):
    wide_rows = rows.astype(jnp.float32)
    scale = lax.rsqrt(jnp.mean(wide_rows * wide_rows, axis=-1, keepdims=True) + norm_eps)
    return (wide_rows * scale * gain).astype(jnp.bfloat16)


def on_device(
    tokens,
    mix_gain,
    w_query,
    w_key,
    w_value,
    w_igate,
    w_fgate,
    igate_bias,
    fgate_bias,
    memory,
    normalizer,
    stabilizer,
    w_output,
    mlp_gain,
    w_up,
    w_down,
):
    DV, DQK = memory.shape[2:]
    kv_count = lax.axis_size("kv")
    tp_count = lax.axis_size("tp")
    kv_index = lax.axis_index("kv")
    tp_index = lax.axis_index("tp")
    own_rows = memory.shape[0]
    head_count = memory.shape[1]
    whole_rows = lax.all_gather(tokens, ("kv", "tp"), axis=1, tiled=True)
    batch_rows = whole_rows.shape[0]
    wide_rows = whole_rows.astype(jnp.float32)
    normed = rms_normed(whole_rows, mix_gain)
    row_span = w_query.shape[0]
    own_cols = lax.dynamic_slice_in_dim(normed, kv_index * row_span, row_span, 1)
    joined = lax.psum_scatter(
        jnp.concatenate(
            [
                jnp.dot(own_cols, w_query, preferred_element_type=jnp.float32),
                jnp.dot(own_cols, w_key, preferred_element_type=jnp.float32),
                jnp.dot(own_cols, w_value, preferred_element_type=jnp.float32),
            ],
            axis=1,
        ),
        "kv",
        scatter_dimension=0,
        tiled=True,
    )
    query_cols = w_query.shape[1]
    queries = joined[:, :query_cols].reshape(own_rows, head_count, DQK) * DQK ** (-0.5)
    key_rows = joined[:, query_cols : 2 * query_cols].reshape(own_rows, head_count, DQK)
    values = joined[:, 2 * query_cols :].reshape(own_rows, head_count, DV)
    own_normed = lax.dynamic_slice_in_dim(normed, kv_index * own_rows, own_rows, 0)
    igate_cols = lax.dynamic_slice_in_dim(w_igate, tp_index * head_count, head_count, 1)
    fgate_cols = lax.dynamic_slice_in_dim(w_fgate, tp_index * head_count, head_count, 1)
    ibias_own = lax.dynamic_slice_in_dim(igate_bias, tp_index * head_count, head_count, 0)
    fbias_own = lax.dynamic_slice_in_dim(fgate_bias, tp_index * head_count, head_count, 0)
    input_gate = jnp.dot(own_normed, igate_cols, preferred_element_type=jnp.float32) + ibias_own
    log_forget = jax.nn.log_sigmoid(
        jnp.dot(own_normed, fgate_cols, preferred_element_type=jnp.float32) + fbias_own
    )
    carried = log_forget + stabilizer
    new_stabilizer = jnp.maximum(carried, input_gate)
    keep_weight = jnp.exp(carried - new_stabilizer)
    fresh_weight = jnp.exp(input_gate - new_stabilizer)
    recall = jnp.einsum("bhvd,bhd->bhv", memory, queries, precision=lax.Precision.HIGHEST)
    match_score = jnp.sum(queries * key_rows, axis=-1)
    numerator = keep_weight[..., None] * recall + (fresh_weight * match_score)[..., None] * values
    denominator = keep_weight * jnp.sum(normalizer * queries, axis=-1) + fresh_weight * match_score
    floor_value = jnp.maximum(jnp.abs(denominator), jnp.exp(-new_stabilizer))
    cell_out = (
        (numerator / floor_value[..., None]).astype(jnp.bfloat16).reshape(own_rows, head_count * DV)
    )
    new_memory = (
        keep_weight[..., None, None] * memory
        + fresh_weight[..., None, None] * values[..., :, None] * key_rows[..., None, :]
    )
    new_normalizer = keep_weight[..., None] * normalizer + fresh_weight[..., None] * key_rows
    partial_value = jnp.dot(
        lax.all_gather(cell_out, "kv", axis=0, tiled=True),
        w_output,
        preferred_element_type=jnp.float32,
    )
    block_cols = partial_value.shape[1]
    pieces = lax.all_gather(
        partial_value.astype(jnp.bfloat16)[:, None, :], ("kv", "tp"), axis=1, tiled=True
    )
    summed = jnp.sum(
        pieces.astype(jnp.float32).reshape(batch_rows, kv_count, tp_count, block_cols), axis=2
    )
    middle = (wide_rows + summed.reshape(batch_rows, kv_count * block_cols)).astype(jnp.bfloat16)
    mixer_in = rms_normed(middle, mlp_gain)
    up_rows = jnp.dot(mixer_in, w_up, preferred_element_type=jnp.float32)
    activation = jnp.square(jax.nn.relu(up_rows)).astype(jnp.bfloat16)
    thin_cols = tokens.shape[1]
    down_cols = lax.psum_scatter(
        lax.dot_general(
            w_down, activation, (((0,), (1,)), ((), ())), preferred_element_type=jnp.float32
        ),
        ("kv", "tp"),
        scatter_dimension=0,
        tiled=True,
    )
    middle_own = lax.dynamic_slice_in_dim(
        middle, (kv_index * tp_count + tp_index) * thin_cols, thin_cols, 1
    )
    new_tokens = (middle_own.astype(jnp.float32) + down_cols.T).astype(jnp.bfloat16)
    return (new_tokens, new_memory, new_normalizer, new_stabilizer)


def fused_cell(
    n_kv,
    n_tp,
    tok_h, mixg_h, wq_h, wk_h, wv_h, wig_h, wfg_h, ib_h, fb_h,
    mem_h, nrm_h, stb_h, wo_h, mlpg_h, wup_h, wdn_h,
    otok, newmem, onrm, ostb,
    tok, tokall, mixg, wq, wk, wv, wig, wfg, ib, fb,
    mem, membf, nrm, stb, wo, mlpg, wup, wdn,
    snd, rcv, cell_own, cell_all, y_own, y_all, mid, act, stage, land,
    small_sem, w_sem, up_sem,
    tok_s, tok_r, rs_s, rs_r, cell_s, cell_r, y_s, y_r, dn_s, dn_r,
):
    dp = lax.axis_index("dp")
    kv = lax.axis_index("kv")
    tp = lax.axis_index("tp")
    n_all = n_kv * n_tp
    g = kv * n_tp + tp
    batch, thin = tok.shape
    span = wq.shape[0]
    heads, dv, dqk = mem.shape
    width = tokall.shape[0] * thin
    halves = dv // LANES

    def peer_of(offset):
        other = (g + offset) % n_all
        return other, (dp, other // n_tp, other % n_tp)

    barrier = pltpu.get_barrier_semaphore()
    for o in range(1, n_all):
        pl.semaphore_signal(barrier, inc=1, device_id=peer_of(o)[1], device_id_type=MESH)

    own_span = pl.ds(pl.multiple_of(kv * span, span), span)
    smalls = [
        (tok_h, tok), (mixg_h, mixg), (wig_h.at[:, own_span], wig), (wfg_h.at[:, own_span], wfg),
        (ib_h, ib), (fb_h, fb), (nrm_h.at[0], nrm), (stb_h, stb), (mlpg_h, mlpg),
    ]
    small = [pltpu.make_async_copy(a, b, small_sem.at[i]) for i, (a, b) in enumerate(smalls)]
    bigs = [(wq_h, wq), (wk_h, wk), (wv_h, wv), (mem_h.at[0], mem), (wo_h, wo), (wdn_h, wdn)]
    big = [pltpu.make_async_copy(a, b, w_sem.at[i]) for i, (a, b) in enumerate(bigs)]
    for c in small:
        c.start()
    for c in big[:5]:
        c.start()

    def up_rows(i):
        if n_kv == 4:
            far_side = kv // 2
            near = kv + far_side * (3 - 2 * kv)
            step = (i + near) % 2 if i < 2 else i
            j = 3 * far_side + (1 - 2 * far_side) * step
        else:
            j = (kv + i) % n_kv
        return j, pl.ds(pl.multiple_of(j * span, span), span)

    def up_copy(i):
        j, rows = up_rows(i)
        return pltpu.make_async_copy(wup_h.at[rows], wup.at[rows], up_sem.at[j])

    small[0].wait()
    pl.semaphore_wait(barrier, n_all - 1)

    def tok_copy(o):
        return pltpu.make_async_remote_copy(
            src_ref=tok, dst_ref=tokall.at[g], send_sem=tok_s.at[o], recv_sem=tok_r.at[g],
            device_id=peer_of(o)[1], device_id_type=MESH)

    def tok_wait(src):
        pltpu.make_async_remote_copy(
            src_ref=tok, dst_ref=tokall.at[src], send_sem=tok_s.at[0], recv_sem=tok_r.at[src],
            device_id=peer_of(1)[1], device_id_type=MESH).wait_recv()

    mate = [(kv * n_tp + (tp + t) % n_tp) for t in range(1, n_tp)]
    for src in mate:
        pltpu.make_async_remote_copy(
            src_ref=tok, dst_ref=tokall.at[g], send_sem=tok_s.at[src], recv_sem=tok_r.at[g],
            device_id=(dp, kv, src % n_tp), device_id_type=MESH).start()
    tokall[g] = tok[...]

    def far_tok(o, t):
        to = (kv + o) % n_kv
        other = to * n_tp + (tp + t) % n_tp
        return other, pltpu.make_async_remote_copy(
            src_ref=tok, dst_ref=tokall.at[g], send_sem=tok_s.at[other], recv_sem=tok_r.at[g],
            device_id=(dp, to, (tp + t) % n_tp), device_id_type=MESH)

    for o in range(1, n_kv):
        for t in range(n_tp):
            far_tok(o, t)[1].start()

    snd[:, heads : 2 * heads, :] = jnp.zeros((n_kv, heads, LANES), F32)
    for c in small[1:]:
        c.wait()

    def chunk(t):
        cols = pl.ds(pl.multiple_of((kv * n_tp + t) * thin, thin), thin)
        raw = tokall[kv * n_tp + t].astype(F32)
        return (raw * mixg[:, cols]).astype(BF16), jnp.sum(raw * raw, axis=1, keepdims=True)

    def product(x, t, w):
        rows = pl.ds(pl.multiple_of(t * thin, thin), thin)
        return jnp.dot(x, w[rows, :], preferred_element_type=F32)

    x_own, squares = chunk(tp)
    for c in big[:3]:
        c.wait()
    for i in range(n_kv):
        up_copy(i).start()
    big[5].start()
    own_parts = [product(x_own, tp, w) for w in (wq, wk, wv)]
    for src in mate:
        tok_wait(src)
    others = [((tp + t) % n_tp, chunk((tp + t) % n_tp)) for t in range(1, n_tp)]
    for _, (_, more) in others:
        squares = squares + more

    def finished(n, w):
        total = own_parts[n]
        for t, (x_t, _) in others:
            total = total + product(x_t, t, w)
        return total

    x = jnp.concatenate([chunk(t)[0] for t in range(n_tp)], axis=1)
    snd[:, heads + 2, :] = jnp.broadcast_to(squares, (n_kv, LANES))
    gate_count = wig.shape[0]
    last = (((1,), (1,)), ((), ()))
    snd[:, heads, :gate_count] = lax.dot_general(x, wig[...], last, preferred_element_type=F32)
    snd[:, heads + 1, :gate_count] = lax.dot_general(x, wfg[...], last, preferred_element_type=F32)

    pieces = [(0, 2 * heads), (2 * heads, heads), (3 * heads, halves * heads)]

    def rs_copy(o, p):
        first, size = pieces[p]
        to = (kv + o) % n_kv
        return pltpu.make_async_remote_copy(
            src_ref=snd.at[to, pl.ds(first, size)],
            dst_ref=rcv.at[o, pl.ds(first, size)],
            send_sem=rs_s.at[o, p], recv_sem=rs_r.at[o, p],
            device_id=(dp, to, tp), device_id_type=MESH)

    far_first = sorted(range(1, n_kv), key=lambda o: -min(o, n_kv - o))
    q_part = finished(0, wq)
    for h in range(heads):
        snd[:, h, :] = q_part[:, h * dqk : (h + 1) * dqk]
    for o in far_first:
        rs_copy(o, 0).start()
    k_part = finished(1, wk)
    for h in range(heads):
        snd[:, 2 * heads + h, :] = k_part[:, h * dqk : (h + 1) * dqk]
    for o in far_first:
        rs_copy(o, 1).start()
    v_part = finished(2, wv)
    for h in range(heads):
        for s in range(halves):
            at = h * dv + s * LANES
            snd[:, (3 + s) * heads + h, :] = v_part[:, at : at + LANES]
    for o in far_first:
        rs_copy(o, 2).start()
    big[3].wait()
    membf[...] = mem[...].astype(BF16).reshape(heads * dv, dqk)

    lane = lax.broadcasted_iota(jnp.int32, (heads, LANES), 1)
    sub = lax.broadcasted_iota(jnp.int32, (heads, LANES), 0)
    own_head = lane == sub + tp * heads

    def column(row):
        wide = jnp.pad(row, ((0, 0), (0, LANES - row.shape[1]))) if row.shape[1] < LANES else row
        return jnp.sum(jnp.where(own_head, jnp.broadcast_to(wide, own_head.shape), 0.0), axis=1, keepdims=True)

    def joined(p):
        first, size = pieces[p]
        total = snd[kv, first : first + size, :]
        for o in range(1, n_kv):
            rs_copy(o, p).wait_recv()
            total = total + rcv[o, first : first + size, :]
        return total

    part = joined(0)
    scale = lax.rsqrt(part[heads + 2 : heads + 3] * (1.0 / width) + norm_eps)
    q = part[:heads] * scale * dqk**-0.5
    gate_i = column(part[heads : heads + 1] * scale) + column(ib[...])
    gate_f = column(part[heads + 1 : heads + 2] * scale) + column(fb[...])
    log_forget = jnp.minimum(gate_f, 0.0) - jnp.log1p(jnp.exp(-jnp.abs(gate_f)))
    stab_wide = jnp.broadcast_to(stb[...], (heads, heads))
    eye = (lax.broadcasted_iota(jnp.int32, (heads, heads), 0)
           == lax.broadcasted_iota(jnp.int32, (heads, heads), 1))
    stab = jnp.sum(jnp.where(eye, stab_wide, 0.0), axis=1, keepdims=True)
    carried = log_forget + stab
    new_stab = jnp.maximum(carried, gate_i)
    keep = jnp.exp(carried - new_stab)
    fresh = jnp.exp(gate_i - new_stab)
    ostb[...] = jnp.sum(jnp.where(eye, jnp.broadcast_to(new_stab, (heads, heads)), 0.0), axis=0, keepdims=True)
    norm_dot = jnp.sum(nrm[...] * q, axis=1, keepdims=True)
    q_hi = q.astype(BF16)
    q_lo = (q - q_hi.astype(F32)).astype(BF16)
    wide_recall = lax.dot_general(
        jnp.concatenate([q_hi, q_lo], axis=0), membf[...], (((1,), (1,)), ((), ())),
        preferred_element_type=F32)
    wide_recall = wide_recall[:heads] + wide_recall[heads:]
    row_id = lax.broadcasted_iota(jnp.int32, (heads, dv), 0)
    recall = jnp.zeros((heads, dv), F32)
    for h in range(heads):
        recall = jnp.where(row_id == h, wide_recall[:, h * dv : (h + 1) * dv], recall)
    k = joined(1) * scale
    match = jnp.sum(q * k, axis=1, keepdims=True)
    denominator = keep * norm_dot + fresh * match
    floor_value = jnp.maximum(jnp.abs(denominator), jnp.exp(-new_stab))
    v_rows = joined(2)
    v = jnp.concatenate([v_rows[s * heads : (s + 1) * heads] * scale for s in range(halves)], axis=1)
    cell = (keep * recall + (fresh * match) * v) / floor_value
    cell = cell.astype(BF16)
    cell_own[...] = cell

    def cell_copy(o):
        to = (kv + o) % n_kv
        return pltpu.make_async_remote_copy(
            src_ref=cell_own, dst_ref=cell_all.at[kv], send_sem=cell_s.at[o], recv_sem=cell_r.at[o],
            device_id=(dp, to, tp), device_id_type=MESH)

    for o in far_first:
        cell_copy(o).start()
    cell_all[kv] = cell
    onrm[0] = keep * nrm[...] + fresh * k
    fresh_v = fresh * v
    fresh_vt = fresh_v.T
    for h in range(heads):
        newmem[0, h] = keep[h : h + 1] * mem[h] + fresh_vt[:, h : h + 1] * k[h : h + 1]
    big[4].wait()
    for o in range(1, n_kv):
        src = (kv + n_kv - o) % n_kv
        pltpu.make_async_remote_copy(
            src_ref=cell_own, dst_ref=cell_all.at[src], send_sem=cell_s.at[o], recv_sem=cell_r.at[o],
            device_id=(dp, src, tp), device_id_type=MESH).wait_recv()
    cells = cell_all[...].astype(F32)
    rows = jnp.concatenate([cells[:, h, :] for h in range(heads)], axis=1).astype(BF16)
    y = jnp.dot(rows, wo[...], preferred_element_type=F32).astype(BF16)
    y_own[...] = y

    def y_copy(o, t):
        to = (kv + o) % n_kv
        to_tp = (tp + t) % n_tp
        return pltpu.make_async_remote_copy(
            src_ref=y_own, dst_ref=y_all.at[g], send_sem=y_s.at[to * n_tp + to_tp], recv_sem=y_r.at[g],
            device_id=(dp, to, to_tp), device_id_type=MESH)

    for o in far_first + [0]:
        for t in range(n_tp):
            if o or t:
                y_copy(o, t).start()
    y_all[g] = y
    for o in range(1, n_kv):
        for t in range(n_tp):
            tok_wait(((kv + o) % n_kv) * n_tp + (tp + t) % n_tp)

    def y_wait(src):
        pltpu.make_async_remote_copy(
            src_ref=y_own, dst_ref=y_all.at[src], send_sem=y_s.at[0], recv_sem=y_r.at[src],
            device_id=peer_of(1)[1], device_id_type=MESH).wait_recv()

    def up_step(i, square_sum, total_up):
        j, span_rows = up_rows(i)
        up_copy(i).wait()
        for t in range(1, n_tp):
            y_wait(j * n_tp + (tp + t) % n_tp)

        if i > 0:
            y_wait(j * n_tp + tp)

        base = jnp.concatenate([tokall[j * n_tp + t].astype(F32) for t in range(n_tp)], axis=1)
        for t in range(n_tp):
            base = base + y_all[j * n_tp + t].astype(F32)
        m = base.astype(BF16).astype(F32)
        mid[j] = m
        mixed = (m * mlpg[:, span_rows]).astype(BF16)
        part = jnp.dot(mixed, wup[span_rows, :], preferred_element_type=F32)

        total_up = part if total_up is None else total_up + part
        return square_sum + jnp.sum(m * m, axis=1, keepdims=True), total_up

    square_sum = jnp.zeros((batch, 1), F32)
    total_up = None
    for i in range(n_kv):
        square_sum, total_up = up_step(i, square_sum, total_up)
    scale2 = lax.rsqrt(square_sum * (1.0 / width) + norm_eps)
    up = jnp.maximum(total_up * scale2, 0.0)
    act[...] = (up * up).astype(BF16)
    big[5].wait()

    def dn_copy(to, src):
        return pltpu.make_async_remote_copy(
            src_ref=stage.at[to], dst_ref=land.at[src], send_sem=dn_s.at[to], recv_sem=dn_r.at[src],
            device_id=(dp, to // n_tp, to % n_tp), device_id_type=MESH)

    targets = [
        up_rows(i)[0] * n_tp + (tp + t) % n_tp
        for i in reversed(range(n_kv)) for t in reversed(range(n_tp))
    ]
    for to in targets[:-1]:
        cols = pl.ds(pl.multiple_of(to * thin, thin), thin)
        stage[to] = jnp.dot(act[...], wdn[:, cols], preferred_element_type=F32)
        dn_copy(to, g).start()
    own_cols = pl.ds(pl.multiple_of(g * thin, thin), thin)
    total = jnp.dot(act[...], wdn[:, own_cols], preferred_element_type=F32)
    total = total + mid[kv, :, pl.ds(pl.multiple_of(tp * thin, thin), thin)]
    for src in reversed(targets[:-1]):
        dn_copy(src, src).wait_recv()
        total = total + land[src]
    otok[...] = total.astype(BF16)

    for src in mate:
        pltpu.make_async_remote_copy(
            src_ref=tok, dst_ref=tokall.at[g], send_sem=tok_s.at[src], recv_sem=tok_r.at[g],
            device_id=(dp, kv, src % n_tp), device_id_type=MESH).wait_send()
    for o in range(n_kv):
        for t in range(n_tp):
            if o:
                far_tok(o, t)[1].wait_send()
            if o or t:
                y_copy(o, t).wait_send()
        if o:
            for p in range(len(pieces)):
                rs_copy(o, p).wait_send()
            cell_copy(o).wait_send()
    for to in targets[:-1]:
        dn_copy(to, g).wait_send()


def hand_over(a, b, c, d, out_a, out_b, out_c, out_d, sems):
    pairs = ((b, out_b), (a, out_a), (c, out_c), (d, out_d))
    copies = [pltpu.make_async_copy(x, y, sems.at[i]) for i, (x, y) in enumerate(pairs)]
    for c in copies:
        c.start()
    for c in copies:
        c.wait()


def fits_fused(tokens, w_query, w_value, memory, w_output, w_up, w_down, n_kv, n_tp):
    own_rows, heads, dv, dqk = memory.shape
    batch, thin = tokens.shape
    span = w_query.shape[0]
    held = 2 * (2 * w_query.size + w_value.size + w_output.size + w_up.size + w_down.size)
    held += 10 * memory.size
    return (
        own_rows == 1 and batch == n_kv and heads == 8 and dqk == LANES and dv % LANES == 0
        and thin % LANES == 0 and span == n_tp * thin and n_kv >= 2 and n_tp >= 2
        and w_output.shape[1] == span and held < 52 * 2**20
    )


def fused_on_device(
    tokens, mix_gain, w_query, w_key, w_value, w_igate, w_fgate, igate_bias, fgate_bias,
    memory, normalizer, stabilizer, w_output, mlp_gain, w_up, w_down,
):
    n_kv = lax.axis_size("kv")
    n_tp = lax.axis_size("tp")
    n_all = n_kv * n_tp
    batch, thin = tokens.shape
    _, heads, dv, dqk = memory.shape
    span = w_query.shape[0]
    width = n_all * thin
    halves = dv // LANES
    groups = (3 + halves) * heads
    hidden = w_up.shape[1]
    hbm_spec = pl.BlockSpec(memory_space=pltpu.HBM)
    vmem_spec = pl.BlockSpec(memory_space=pltpu.VMEM)
    vm = pltpu.VMEM
    dma = pltpu.SemaphoreType.DMA
    scratch = [
        vm((batch, thin), BF16),
        vm((n_all, batch, thin), BF16),
        vm((1, width), F32),
        vm(w_query.shape, BF16),
        vm(w_key.shape, BF16),
        vm(w_value.shape, BF16),
        vm((w_igate.shape[1], span), BF16),
        vm((w_fgate.shape[1], span), BF16),
        vm((1, igate_bias.shape[0]), F32),
        vm((1, fgate_bias.shape[0]), F32),
        vm((heads, dv, dqk), F32),
        vm((heads * dv, dqk), BF16),
        vm((heads, dqk), F32),
        vm((1, heads), F32),
        vm(w_output.shape, BF16),
        vm((1, width), F32),
        vm(w_up.shape, BF16),
        vm(w_down.shape, BF16),
        vm((n_kv, groups, LANES), F32),
        vm((n_kv, groups, LANES), F32),
        vm((heads, dv), BF16),
        vm((n_kv, heads, dv), BF16),
        vm((batch, span), BF16),
        vm((n_all, batch, span), BF16),
        vm((n_kv, batch, span), F32),
        vm((batch, hidden), BF16),
        vm((n_all, batch, thin), F32),
        vm((n_all, batch, thin), F32),
        dma((9,)), dma((6,)), dma((n_kv,)),
        dma((n_all,)), dma((n_all,)),
        dma((n_kv, 3)), dma((n_kv, 3)),
        dma((n_kv,)), dma((n_kv,)),
        dma((n_all,)), dma((n_all,)),
        dma((n_all,)), dma((n_all,)),
    ]
    args = (
        tokens, mix_gain.reshape(1, -1), w_query, w_key, w_value, w_igate.T, w_fgate.T,
        igate_bias.reshape(1, -1), fgate_bias.reshape(1, -1), memory, normalizer, stabilizer,
        w_output, mlp_gain.reshape(1, -1), w_up, w_down,
    )
    args = [pltpu.with_memory_space_constraint(a, pltpu.HBM) for a in args]
    results = pl.pallas_call(
        functools.partial(fused_cell, n_kv, n_tp),
        out_shape=(
            jax.ShapeDtypeStruct(tokens.shape, BF16),
            jax.ShapeDtypeStruct(memory.shape, F32),
            jax.ShapeDtypeStruct(normalizer.shape, F32),
            jax.ShapeDtypeStruct(stabilizer.shape, F32),
        ),
        in_specs=[hbm_spec] * 16,
        out_specs=(vmem_spec,) * 4,
        scratch_shapes=scratch,
        compiler_params=pltpu.CompilerParams(
            collective_id=0, has_side_effects=True, vmem_limit_bytes=52 * 2**20
        ),
        name="fused_cell",
    )(*args)
    return pl.pallas_call(
        hand_over,
        out_shape=tuple(jax.ShapeDtypeStruct(r.shape, r.dtype) for r in results),
        in_specs=[vmem_spec] * 4,
        out_specs=(hbm_spec,) * 4,
        scratch_shapes=[dma((4,))],
        compiler_params=pltpu.CompilerParams(vmem_limit_bytes=2**20),
        name="hand_over",
    )(*results)


def routed(*arrays):
    tokens, w_query, w_value, memory = arrays[0], arrays[2], arrays[4], arrays[9]
    w_output, w_up, w_down = arrays[12], arrays[14], arrays[15]
    n_kv, n_tp = lax.axis_size("kv"), lax.axis_size("tp")
    if fits_fused(tokens, w_query, w_value, memory, w_output, w_up, w_down, n_kv, n_tp):
        return fused_on_device(*arrays)
    return on_device(*arrays)


def solution(mesh):
    in_specs = (
        P("dp", ("kv", "tp")),
        P(),
        P("kv", "tp"),
        P("kv", "tp"),
        P("kv", "tp"),
        P(),
        P(),
        P(),
        P(),
        P(("dp", "kv"), "tp", None, None),
        P(("dp", "kv"), "tp", None),
        P(("dp", "kv"), "tp"),
        P("tp", "kv"),
        P(),
        P(None, ("kv", "tp")),
        P(("kv", "tp"), None),
    )
    out_specs = (
        P("dp", ("kv", "tp")),
        P(("dp", "kv"), "tp", None, None),
        P(("dp", "kv"), "tp", None),
        P(("dp", "kv"), "tp"),
    )
    return jax.shard_map(
        routed, mesh=mesh, in_specs=in_specs, out_specs=out_specs, check_vma=False
    )
```

profile of v0, /device:TPU:0, one launch (start us, length us, event | category | flops | bytes accessed | tf_op | source)
XLA Modules:
  0.0 28.6 jit_solution(17155396232808944564)
XLA Ops:
  0.6 26.9 %fused_cell.1 = (bf16[4,512]{1,0:T(4,128)(2,1)S(1)}, f32[1,8,256,128]{3,2,1,0:T(8,128)S(1)}, f32[1,8,128]{2,1,0:T(8,128)S(1)}, f32[1,8]{1,0:T(1,128)S(1)}) custom-call(bf16[4,512]{1,0:T(4,128)(2,1)} %tok_h.1, f32[1,4096]{1,0:T(1,128)} %bitcast.8, bf16[1024,1024]{1,0:T(8,128)(2,1)} %wq_h.1, bf16[1024,1024]{1,0:T(8,128)(2,1)} %wk_h.1, ...), custom_call_target="tpu_custom_call" | custom-call | tf_op jit(solution)/shard_map/fused_cell/pallas_call | solution.py:539
  27.5 1.0 %hand_over.1 = (bf16[4,512]{1,0:T(4,128)(2,1)}, f32[1,8,256,128]{3,2,1,0:T(8,128)}, f32[1,8,128]{2,1,0:T(8,128)}, f32[1,8]{1,0:T(1,128)}) custom-call(bf16[4,512]{1,0:T(4,128)(2,1)S(1)} %get-tuple-element.8.a, f32[1,8,256,128]{3,2,1,0:T(8,128)S(1)} %get-tuple-element.9.b, f32[1,8,128]{2,1,0:T(8,128)S(1)} %get-tuple-element.10.c, f32[1,8]{1,0:T(1,128)S(1)} %get-tuple-element.11.d), custom_call_target="tpu_custom_call" | custom-call | tf_op jit(solution)/shard_map/hand_over/pallas_call | solution.py:555
where the time goes:
time: 28.7 us; the launch traced here: 28.6 us
  Pallas kernels  27.9 us (97%)
  between operations  0.65 us (2%)
    pallas_call x1, Pallas kernels, fused_on_device(): pl.pallas_call(functools.partial(fused_cell, n_kv, n_tp), out_shape=(jax....  26.9 us
    pallas_call x1, Pallas kernels, fused_on_device(): pl.pallas_call(hand_over, out_shape=tuple((jax.ShapeDtypeStruct(r.shape,...  1.01 us

commit v1 on v0

v1 whole, which is shorter than its diff:
```python
import functools

import jax
import jax.numpy as jnp
from jax import lax
from jax.experimental import pallas as pl
from jax.experimental.pallas import tpu as pltpu
from jax.sharding import PartitionSpec as P

MESH = pl.DeviceIdType.MESH
F32 = jnp.float32
BF16 = jnp.bfloat16
LANES = 128


norm_eps = 1e-06


def rms_normed(rows, gain):
    wide_rows = rows.astype(jnp.float32)
    scale = lax.rsqrt(jnp.mean(wide_rows * wide_rows, axis=-1, keepdims=True) + norm_eps)
    return (wide_rows * scale * gain).astype(jnp.bfloat16)


def on_device(
    tokens,
    mix_gain,
    w_query,
    w_key,
    w_value,
    w_igate,
    w_fgate,
    igate_bias,
    fgate_bias,
    memory,
    normalizer,
    stabilizer,
    w_output,
    mlp_gain,
    w_up,
    w_down,
):
    DV, DQK = memory.shape[2:]
    kv_count = lax.axis_size("kv")
    tp_count = lax.axis_size("tp")
    kv_index = lax.axis_index("kv")
    tp_index = lax.axis_index("tp")
    own_rows = memory.shape[0]
    head_count = memory.shape[1]
    whole_rows = lax.all_gather(tokens, ("kv", "tp"), axis=1, tiled=True)
    batch_rows = whole_rows.shape[0]
    wide_rows = whole_rows.astype(jnp.float32)
    normed = rms_normed(whole_rows, mix_gain)
    row_span = w_query.shape[0]
    own_cols = lax.dynamic_slice_in_dim(normed, kv_index * row_span, row_span, 1)
    joined = lax.psum_scatter(
        jnp.concatenate(
            [
                jnp.dot(own_cols, w_query, preferred_element_type=jnp.float32),
                jnp.dot(own_cols, w_key, preferred_element_type=jnp.float32),
                jnp.dot(own_cols, w_value, preferred_element_type=jnp.float32),
            ],
            axis=1,
        ),
        "kv",
        scatter_dimension=0,
        tiled=True,
    )
    query_cols = w_query.shape[1]
    queries = joined[:, :query_cols].reshape(own_rows, head_count, DQK) * DQK ** (-0.5)
    key_rows = joined[:, query_cols : 2 * query_cols].reshape(own_rows, head_count, DQK)
    values = joined[:, 2 * query_cols :].reshape(own_rows, head_count, DV)
    own_normed = lax.dynamic_slice_in_dim(normed, kv_index * own_rows, own_rows, 0)
    igate_cols = lax.dynamic_slice_in_dim(w_igate, tp_index * head_count, head_count, 1)
    fgate_cols = lax.dynamic_slice_in_dim(w_fgate, tp_index * head_count, head_count, 1)
    ibias_own = lax.dynamic_slice_in_dim(igate_bias, tp_index * head_count, head_count, 0)
    fbias_own = lax.dynamic_slice_in_dim(fgate_bias, tp_index * head_count, head_count, 0)
    input_gate = jnp.dot(own_normed, igate_cols, preferred_element_type=jnp.float32) + ibias_own
    log_forget = jax.nn.log_sigmoid(
        jnp.dot(own_normed, fgate_cols, preferred_element_type=jnp.float32) + fbias_own
    )
    carried = log_forget + stabilizer
    new_stabilizer = jnp.maximum(carried, input_gate)
    keep_weight = jnp.exp(carried - new_stabilizer)
    fresh_weight = jnp.exp(input_gate - new_stabilizer)
    recall = jnp.einsum("bhvd,bhd->bhv", memory, queries, precision=lax.Precision.HIGHEST)
    match_score = jnp.sum(queries * key_rows, axis=-1)
    numerator = keep_weight[..., None] * recall + (fresh_weight * match_score)[..., None] * values
    denominator = keep_weight * jnp.sum(normalizer * queries, axis=-1) + fresh_weight * match_score
    floor_value = jnp.maximum(jnp.abs(denominator), jnp.exp(-new_stabilizer))
    cell_out = (
        (numerator / floor_value[..., None]).astype(jnp.bfloat16).reshape(own_rows, head_count * DV)
    )
    new_memory = (
        keep_weight[..., None, None] * memory
        + fresh_weight[..., None, None] * values[..., :, None] * key_rows[..., None, :]
    )
    new_normalizer = keep_weight[..., None] * normalizer + fresh_weight[..., None] * key_rows
    partial_value = jnp.dot(
        lax.all_gather(cell_out, "kv", axis=0, tiled=True),
        w_output,
        preferred_element_type=jnp.float32,
    )
    block_cols = partial_value.shape[1]
    pieces = lax.all_gather(
        partial_value.astype(jnp.bfloat16)[:, None, :], ("kv", "tp"), axis=1, tiled=True
    )
    summed = jnp.sum(
        pieces.astype(jnp.float32).reshape(batch_rows, kv_count, tp_count, block_cols), axis=2
    )
    middle = (wide_rows + summed.reshape(batch_rows, kv_count * block_cols)).astype(jnp.bfloat16)
    mixer_in = rms_normed(middle, mlp_gain)
    up_rows = jnp.dot(mixer_in, w_up, preferred_element_type=jnp.float32)
    activation = jnp.square(jax.nn.relu(up_rows)).astype(jnp.bfloat16)
    thin_cols = tokens.shape[1]
    down_cols = lax.psum_scatter(
        lax.dot_general(
            w_down, activation, (((0,), (1,)), ((), ())), preferred_element_type=jnp.float32
        ),
        ("kv", "tp"),
        scatter_dimension=0,
        tiled=True,
    )
    middle_own = lax.dynamic_slice_in_dim(
        middle, (kv_index * tp_count + tp_index) * thin_cols, thin_cols, 1
    )
    new_tokens = (middle_own.astype(jnp.float32) + down_cols.T).astype(jnp.bfloat16)
    return (new_tokens, new_memory, new_normalizer, new_stabilizer)


def landed(ref, sem):
    pltpu.make_async_copy(ref, ref, sem).wait()


def fused_cell(
    n_kv,
    n_tp,
    tok_h, mixg_h, wq_h, wk_h, wv_h, wig_h, wfg_h, ib_h, fb_h,
    mem_h, nrm_h, stb_h, wo_h, mlpg_h, wup_h, wdn_h,
    otok, newmem, onrm, ostb,
    tok, tokall, gains, wq, wk, wv, wg, bias,
    mem, membf, nrm, stb, wo, wup, wdn,
    own_part, part, snd, rcv, gsnd, grcv, vrow, cell_own, cell_all, y_own, y_all, mid, stage, land,
    load_sem, sent_sem, tok_r, rs_r, cell_r, y_r, dn_r,
):
    dp = lax.axis_index("dp")
    kv = lax.axis_index("kv")
    tp = lax.axis_index("tp")
    n_all = n_kv * n_tp
    g = kv * n_tp + tp
    batch, thin = tok.shape
    span = wq.shape[0]
    heads, dv, dqk = mem.shape
    width = n_all * thin
    halves = dv // LANES
    gate_count = wg.shape[0] // 2
    block = heads * LANES
    hidden = wup.shape[1]
    TOK_S, RS_S, GATE_S, CELL_S, Y_S, DN_S = range(6)

    def peer_of(offset):
        other = (g + offset) % n_all
        return dp, other // n_tp, other % n_tp

    own_span = pl.ds(pl.multiple_of(kv * span, span), span)

    def v_cols(p):
        return pl.ds(p * block, block)

    far_side = kv // 2
    near = kv + far_side * (3 - 2 * kv)

    def chip(i):
        if n_kv == 4:
            step = (i + near) % 3 if i < 3 else i
            return 3 * far_side + (1 - 2 * far_side) * step
        return (kv + i) % n_kv

    chips = [chip(i) for i in range(n_kv)]
    far_first = chips[:0:-1]

    def up_rows(j):
        return pl.ds(pl.multiple_of(j * span, span), span)

    TOK, GAINS, WQ, WK, WG, BIAS, NRM, STB, MEM, WO, WUP, WDN, WV = range(13)
    loads = [
        (tok_h, tok, TOK), (mixg_h, gains.at[0], GAINS), (mlpg_h, gains.at[1], GAINS), (wq_h, wq, WQ),
        (wk_h, wk, WK),
        (wig_h.at[:, own_span], wg.at[pl.ds(0, gate_count)], WG),
        (wfg_h.at[:, own_span], wg.at[pl.ds(gate_count, gate_count)], WG),
    ]
    loads += [(wv_h.at[:, v_cols(p)], wv.at[:, v_cols(p)], WV + p) for p in range(halves)]
    loads += [
        (ib_h, bias.at[0], BIAS), (fb_h, bias.at[1], BIAS), (nrm_h.at[0], nrm, NRM), (stb_h, stb, STB),
        (mem_h.at[0], mem, MEM), (wo_h, wo, WO),
    ]
    loads += [(wup_h.at[up_rows(j)], wup.at[up_rows(j)], WUP) for j in chips]
    loads += [(wdn_h, wdn, WDN)]
    load = [pltpu.make_async_copy(x, y, load_sem.at[n]) for x, y, n in loads]

    for c in load[:4]:
        c.start()
    barrier = pltpu.get_barrier_semaphore()
    for o in reversed(range(1, n_all)):
        pl.semaphore_signal(barrier, inc=1, device_id=peer_of(o), device_id_type=MESH)
    for c in load[4:]:
        c.start()

    gsnd[...] = jnp.zeros(gsnd.shape, F32)
    landed(tok, load_sem.at[TOK])
    pl.semaphore_wait(barrier, n_all - 1)

    def tok_copy(to, to_tp, n):
        return pltpu.make_async_remote_copy(
            src_ref=tok, dst_ref=tokall.at[g], send_sem=sent_sem.at[TOK_S], recv_sem=tok_r.at[n],
            device_id=(dp, to, to_tp), device_id_type=MESH)

    for t in range(1, n_tp):
        tok_copy(kv, (tp + t) % n_tp, 0).start()
    tokall[g] = tok[...]
    for to in far_first:
        for t in range(n_tp):
            tok_copy(to, (tp + t) % n_tp, 1).start()

    def chunk(t):
        cols = pl.ds(pl.multiple_of((kv * n_tp + t) * thin, thin), thin)
        raw = tokall[kv * n_tp + t].astype(F32)
        return (raw * gains[0, :, cols]).astype(BF16), jnp.sum(raw * raw, axis=1, keepdims=True)

    def product(x, t, w, cols):
        rows = pl.ds(pl.multiple_of(t * thin, thin), thin)
        return jnp.dot(x, w[rows, cols], preferred_element_type=F32)

    last = (((1,), (1,)), ((), ()))

    def gate_part(x, t):
        rows = pl.ds(pl.multiple_of(t * thin, thin), thin)
        return lax.dot_general(x, wg[:, rows], last, preferred_element_type=F32)

    whole = pl.ds(0, block)
    columns_of = [(wq, whole, WQ), (wk, whole, WK)] + [(wv, v_cols(p), WV + p) for p in range(halves)]
    early = 3
    landed(gains, load_sem.at[GAINS])
    x_own, squares = chunk(tp)
    pending = None
    for n, (w, cols, sem) in enumerate(columns_of[:early]):
        landed(w.at[:, cols], load_sem.at[sem])
        made = product(x_own, tp, w, cols)
        if pending is not None:
            own_part[n - 1] = pending
        pending = made
    landed(wg, load_sem.at[WG])
    gates_own = gate_part(x_own, tp)
    own_part[early - 1] = pending
    gsnd[:, 0, : 2 * gate_count] = gates_own
    landed(tokall.at[pl.ds(0, n_tp - 1)], tok_r.at[0])
    others = [((tp + t) % n_tp, chunk((tp + t) % n_tp)) for t in range(1, n_tp)]
    for _, (_, more) in others:
        squares = squares + more

    def rs_copy(to, p):
        return pltpu.make_async_remote_copy(
            src_ref=snd.at[to, p], dst_ref=rcv.at[kv, p],
            send_sem=sent_sem.at[RS_S], recv_sem=rs_r.at[min(p, 2)],
            device_id=(dp, to, tp), device_id_type=MESH)

    def gate_copy(to):
        return pltpu.make_async_remote_copy(
            src_ref=gsnd.at[to], dst_ref=grcv.at[kv],
            send_sem=sent_sem.at[GATE_S], recv_sem=rs_r.at[3],
            device_id=(dp, to, tp), device_id_type=MESH)

    def send_part(p, total):
        for h in range(heads):
            part[:, p * heads + h, :] = total[:, h * LANES : (h + 1) * LANES]
        for to in range(n_kv):
            snd[to, p] = part[to, p * heads : (p + 1) * heads, :].astype(BF16)
        for to in far_first:
            rs_copy(to, p).start()

    def mate_sum(of):
        total = None
        for t, (x_t, _) in others:
            made = of(x_t, t)
            total = made if total is None else total + made
        return total

    def mate_part(p):
        w, cols, _ = columns_of[p]
        return mate_sum(lambda x_t, t: product(x_t, t, w, cols))

    pending = mate_part(0)
    for p in range(1, len(columns_of)):
        w, cols, sem = columns_of[p]
        if p < early:
            made = mate_part(p)
        else:
            landed(w.at[:, cols], load_sem.at[sem])
            made = product(x_own, tp, w, cols)
        if p == early - 1:
            gates_mate = mate_sum(gate_part)
        send_part(p - 1, pending + own_part[p - 1])
        if p == early - 1:
            gsnd[:, 0, : 2 * gate_count] = gsnd[:, 0, : 2 * gate_count] + gates_mate
            gsnd[:, 1, :] = jnp.broadcast_to(squares, (n_kv, LANES))
            for to in far_first:
                gate_copy(to).start()
        pending = made if p < early else made + mate_part(p)
    send_part(len(columns_of) - 1, pending)

    landed(bias, load_sem.at[BIAS])
    landed(nrm, load_sem.at[NRM])
    landed(stb, load_sem.at[STB])
    landed(mem, load_sem.at[MEM])
    membf[...] = mem[...].astype(BF16).reshape(heads * dv, dqk)

    lane = lax.broadcasted_iota(jnp.int32, (heads, LANES), 1)
    sub = lax.broadcasted_iota(jnp.int32, (heads, LANES), 0)
    own_head = sub + tp * heads

    def column(row, at):
        wide = jnp.pad(row, ((0, 0), (0, LANES - row.shape[1]))) if row.shape[1] < LANES else row
        picked = jnp.where(lane == own_head + at, jnp.broadcast_to(wide, lane.shape), 0.0)
        return jnp.sum(picked, axis=1, keepdims=True)

    peers = [(kv + o) % n_kv for o in range(1, n_kv)]

    def joined(p):
        total = part[kv, p * heads : (p + 1) * heads, :]
        for o in peers:
            total = total + rcv[o, p].astype(F32)
        return total

    landed(grcv.at[pl.ds(0, n_kv - 1)], rs_r.at[3])
    gate_sum = gsnd[kv]
    for o in peers:
        gate_sum = gate_sum + grcv[o]
    scale = lax.rsqrt(gate_sum[1:2] * (1.0 / width) + norm_eps)
    gate_row = gate_sum[0:1] * scale
    gate_i = column(gate_row, 0) + column(bias[0], 0)
    gate_f = column(gate_row, gate_count) + column(bias[1], 0)
    landed(rcv.at[pl.ds(0, n_kv - 1), 0], rs_r.at[0])
    q = joined(0) * scale * dqk**-0.5
    log_forget = jnp.minimum(gate_f, 0.0) - jnp.log1p(jnp.exp(-jnp.abs(gate_f)))
    stab_wide = jnp.broadcast_to(stb[...], (heads, heads))
    eye = (lax.broadcasted_iota(jnp.int32, (heads, heads), 0)
           == lax.broadcasted_iota(jnp.int32, (heads, heads), 1))
    stab = jnp.sum(jnp.where(eye, stab_wide, 0.0), axis=1, keepdims=True)
    carried = log_forget + stab
    new_stab = jnp.maximum(carried, gate_i)
    keep = jnp.exp(carried - new_stab)
    fresh = jnp.exp(gate_i - new_stab)
    ostb[...] = jnp.sum(jnp.where(eye, jnp.broadcast_to(new_stab, (heads, heads)), 0.0), axis=0, keepdims=True)
    norm_dot = jnp.sum(nrm[...] * q, axis=1, keepdims=True)
    q_hi = q.astype(BF16)
    q_lo = (q - q_hi.astype(F32)).astype(BF16)
    wide_recall = lax.dot_general(
        jnp.concatenate([q_hi, q_lo], axis=0), membf[...], (((1,), (1,)), ((), ())),
        preferred_element_type=F32)
    wide_recall = wide_recall[:heads] + wide_recall[heads:]
    row_id = lax.broadcasted_iota(jnp.int32, (heads, dv), 0)
    recall = jnp.zeros((heads, dv), F32)
    for h in range(heads):
        recall = jnp.where(row_id == h, wide_recall[:, h * dv : (h + 1) * dv], recall)
    landed(rcv.at[pl.ds(0, n_kv - 1), 1], rs_r.at[1])
    k = joined(1) * scale
    match = jnp.sum(q * k, axis=1, keepdims=True)
    denominator = keep * norm_dot + fresh * match
    floor_value = jnp.maximum(jnp.abs(denominator), jnp.exp(-new_stab))
    landed(rcv.at[pl.ds(0, n_kv - 1), pl.ds(2, halves)], rs_r.at[2])
    for p in range(halves):
        vrow[p * heads : (p + 1) * heads, :] = joined(2 + p) * scale
    v = jnp.concatenate([vrow[pl.ds(s, heads, stride=halves), :] for s in range(halves)], axis=1)
    cell = (keep * recall + (fresh * match) * v) / floor_value
    cell = cell.astype(BF16)
    cell_own[...] = cell

    for to in far_first:
        pltpu.make_async_remote_copy(
            src_ref=cell_own, dst_ref=cell_all.at[kv], send_sem=sent_sem.at[CELL_S], recv_sem=cell_r.at[0],
            device_id=(dp, to, tp), device_id_type=MESH).start()
    cell_all[kv] = cell
    onrm[0] = keep * nrm[...] + fresh * k
    fresh_v = fresh * v
    fresh_vt = fresh_v.T
    for h in range(heads):
        newmem[0, h] = keep[h : h + 1] * mem[h] + fresh_vt[:, h : h + 1] * k[h : h + 1]
    landed(wo, load_sem.at[WO])
    landed(wup, load_sem.at[WUP])
    landed(tokall.at[pl.ds(0, n_all - n_tp)], tok_r.at[1])
    landed(cell_all.at[pl.ds(0, n_kv - 1)], cell_r.at[0])
    cells = cell_all[...].astype(F32)
    rows = jnp.concatenate([cells[:, h, :] for h in range(heads)], axis=1).astype(BF16)

    def lagged(jobs):
        pending = None
        for make, finish in jobs:
            made = make()
            if pending is not None:
                pending[1](pending[0])
            pending = made, finish
        pending[1](pending[0])

    def send_y(c):
        def finish(total):
            y = total.astype(BF16)
            y_own[c] = y
            for to in far_first + [kv]:
                for t in range(n_tp):
                    if t or to is not kv:
                        to_tp = (tp + t) % n_tp
                        pltpu.make_async_remote_copy(
                            src_ref=y_own.at[c], dst_ref=y_all.at[g, c],
                            send_sem=sent_sem.at[Y_S], recv_sem=y_r.at[kv, c],
                            device_id=(dp, to, to_tp), device_id_type=MESH).start()
            y_all[g, c] = y

        return finish

    def y_job(c):
        cols = slice(c * thin, (c + 1) * thin)
        return lambda: jnp.dot(rows, wo[:, cols], preferred_element_type=F32), send_y(c)

    lagged([y_job(c) for c in range(n_tp)])

    square_sum = jnp.zeros((batch, 1), F32)
    total_up = [None, None]
    cut = hidden // 2
    for i, j in enumerate(chips):
        if i == n_kv - 1:
            landed(wdn, load_sem.at[WDN])
        for wanted in ([list(range(n_tp))] if i < n_kv - 1 else [[c] for c in range(n_tp)]):
            mixed = []
            for c in wanted:
                count = n_tp if i > 0 else n_tp - 1
                landed(y_all.at[pl.ds(0, count), c], y_r.at[j, c])
                base = tokall[j * n_tp + c].astype(F32)
                for t in range(n_tp):
                    base = base + y_all[j * n_tp + t, c].astype(F32)
                m = base.astype(BF16).astype(F32)
                if i == 0:
                    mid[c] = m
                cols = pl.ds(pl.multiple_of((j * n_tp + c) * thin, thin), thin)
                mixed.append((m * gains[1, :, cols]).astype(BF16))
                square_sum = square_sum + jnp.sum(m * m, axis=1, keepdims=True)
            at = pl.multiple_of((j * n_tp + wanted[0]) * thin, thin)
            wide = jnp.concatenate(mixed, axis=1) if len(mixed) > 1 else mixed[0]
            for s in range(2):
                more = jnp.dot(
                    wide, wup[pl.ds(at, len(wanted) * thin), s * cut : (s + 1) * cut],
                    preferred_element_type=F32)
                total_up[s] = more if total_up[s] is None else total_up[s] + more
    scale2 = lax.rsqrt(square_sum * (1.0 / width) + norm_eps)

    def activated(total):
        up = jnp.maximum(total * scale2, 0.0)
        return (up * up).astype(BF16)

    targets = [chips[i] * n_tp + (tp + t) % n_tp for i in reversed(range(n_kv)) for t in reversed(range(n_tp))]

    def send_down(to):
        def finish(total):
            stage[to] = total.astype(BF16)
            pltpu.make_async_remote_copy(
                src_ref=stage.at[to], dst_ref=land.at[g],
                send_sem=sent_sem.at[DN_S], recv_sem=dn_r.at[0],
                device_id=(dp, to // n_tp, to % n_tp), device_id_type=MESH).start()

        return finish

    own_down = []
    act_low, act_high = activated(total_up[0]), activated(total_up[1])

    def down_job(n, to):
        def make():
            cols = pl.ds(pl.multiple_of(to * thin, thin), thin)
            low = jnp.dot(act_low, wdn[:cut, cols], preferred_element_type=F32)
            return low + jnp.dot(act_high, wdn[cut:, cols], preferred_element_type=F32)

        return make, send_down(to) if n < len(targets) - 1 else own_down.append

    lagged([down_job(n, to) for n, to in enumerate(targets)])
    total = own_down[0] + mid[tp]

    landed(tokall.at[pl.ds(0, n_all - 1)], sent_sem.at[TOK_S])
    landed(snd.at[pl.ds(0, n_kv - 1)], sent_sem.at[RS_S])
    landed(gsnd.at[pl.ds(0, n_kv - 1)], sent_sem.at[GATE_S])
    landed(cell_all.at[pl.ds(0, n_kv - 1)], sent_sem.at[CELL_S])
    landed(y_all.at[pl.ds(0, n_all - 1)], sent_sem.at[Y_S])
    landed(land.at[pl.ds(0, n_all - 1)], dn_r.at[0])
    for o in range(1, n_all):
        total = total + land[(g + o) % n_all].astype(F32)
    otok[...] = total.astype(BF16)
    landed(stage.at[pl.ds(0, n_all - 1)], sent_sem.at[DN_S])


def hand_over(a, b, c, d, out_a, out_b, out_c, out_d, sems):
    pairs = ((b, out_b), (a, out_a), (c, out_c), (d, out_d))
    copies = [pltpu.make_async_copy(x, y, sems.at[i]) for i, (x, y) in enumerate(pairs)]
    for c in copies:
        c.start()
    for c in copies:
        c.wait()


def fits_fused(tokens, w_query, w_value, memory, w_output, w_up, w_down, n_kv, n_tp):
    own_rows, heads, dv, dqk = memory.shape
    batch, thin = tokens.shape
    span = w_query.shape[0]
    held = 2 * (2 * w_query.size + w_value.size + w_output.size + w_up.size + w_down.size)
    held += 10 * memory.size
    return (
        own_rows == 1 and batch == n_kv and heads == 8 and dqk == LANES and dv % LANES == 0
        and w_query.shape[1] == heads * dqk and w_value.shape[1] == heads * dv
        and thin % (2 * LANES) == 0 and span == n_tp * thin and n_kv >= 2 and n_tp >= 2
        and w_output.shape[1] == span and held < 52 * 2**20
    )


def fused_on_device(
    tokens, mix_gain, w_query, w_key, w_value, w_igate, w_fgate, igate_bias, fgate_bias,
    memory, normalizer, stabilizer, w_output, mlp_gain, w_up, w_down,
):
    n_kv = lax.axis_size("kv")
    n_tp = lax.axis_size("tp")
    n_all = n_kv * n_tp
    batch, thin = tokens.shape
    _, heads, dv, dqk = memory.shape
    span = w_query.shape[0]
    width = n_all * thin
    halves = dv // LANES
    hbm_spec = pl.BlockSpec(memory_space=pltpu.HBM)
    vmem_spec = pl.BlockSpec(memory_space=pltpu.VMEM)
    vm = pltpu.VMEM
    dma = pltpu.SemaphoreType.DMA
    scratch = [
        vm((batch, thin), BF16),
        vm((n_all, batch, thin), BF16),
        vm((2, 1, width), F32),
        vm(w_query.shape, BF16),
        vm(w_key.shape, BF16),
        vm(w_value.shape, BF16),
        vm((2 * w_igate.shape[1], span), BF16),
        vm((2, 1, igate_bias.shape[0]), F32),
        vm((heads, dv, dqk), F32),
        vm((heads * dv, dqk), BF16),
        vm((heads, dqk), F32),
        vm((1, heads), F32),
        vm(w_output.shape, BF16),
        vm(w_up.shape, BF16),
        vm(w_down.shape, BF16),
        vm((3, batch, heads * LANES), F32),
        vm((n_kv, (2 + halves) * heads, LANES), F32),
        vm((n_kv, 2 + halves, heads, LANES), BF16),
        vm((n_kv, 2 + halves, heads, LANES), BF16),
        vm((n_kv, 2, LANES), F32),
        vm((n_kv, 2, LANES), F32),
        vm((halves * heads, LANES), F32),
        vm((heads, dv), BF16),
        vm((n_kv, heads, dv), BF16),
        vm((n_tp, batch, thin), BF16),
        vm((n_all, n_tp, batch, thin), BF16),
        vm((n_tp, batch, thin), F32),
        vm((n_all, batch, thin), BF16),
        vm((n_all, batch, thin), BF16),
        dma((12 + halves,)), dma((6,)),
        dma((2,)), dma((4,)), dma((1,)), dma((n_kv, n_tp)), dma((1,)),
    ]
    args = (
        tokens, mix_gain.reshape(1, -1), w_query, w_key, w_value, w_igate.T, w_fgate.T,
        igate_bias.reshape(1, -1), fgate_bias.reshape(1, -1), memory, normalizer, stabilizer,
        w_output, mlp_gain.reshape(1, -1), w_up, w_down,
    )
    args = [pltpu.with_memory_space_constraint(a, pltpu.HBM) for a in args]
    results = pl.pallas_call(
        functools.partial(fused_cell, n_kv, n_tp),
        out_shape=(
            jax.ShapeDtypeStruct(tokens.shape, BF16),
            jax.ShapeDtypeStruct(memory.shape, F32),
            jax.ShapeDtypeStruct(normalizer.shape, F32),
            jax.ShapeDtypeStruct(stabilizer.shape, F32),
        ),
        in_specs=[hbm_spec] * 16,
        out_specs=(vmem_spec,) * 4,
        scratch_shapes=scratch,
        compiler_params=pltpu.CompilerParams(
            collective_id=0, has_side_effects=True, vmem_limit_bytes=52 * 2**20
        ),
        name="fused_cell",
    )(*args)
    return pl.pallas_call(
        hand_over,
        out_shape=tuple(jax.ShapeDtypeStruct(r.shape, r.dtype) for r in results),
        in_specs=[vmem_spec] * 4,
        out_specs=(hbm_spec,) * 4,
        scratch_shapes=[dma((4,))],
        compiler_params=pltpu.CompilerParams(vmem_limit_bytes=2**20),
        name="hand_over",
    )(*results)


def routed(*arrays):
    tokens, w_query, w_value, memory = arrays[0], arrays[2], arrays[4], arrays[9]
    w_output, w_up, w_down = arrays[12], arrays[14], arrays[15]
    n_kv, n_tp = lax.axis_size("kv"), lax.axis_size("tp")
    if fits_fused(tokens, w_query, w_value, memory, w_output, w_up, w_down, n_kv, n_tp):
        return fused_on_device(*arrays)
    return on_device(*arrays)


def solution(mesh):
    in_specs = (
        P("dp", ("kv", "tp")),
        P(),
        P("kv", "tp"),
        P("kv", "tp"),
        P("kv", "tp"),
        P(),
        P(),
        P(),
        P(),
        P(("dp", "kv"), "tp", None, None),
        P(("dp", "kv"), "tp", None),
        P(("dp", "kv"), "tp"),
        P("tp", "kv"),
        P(),
        P(None, ("kv", "tp")),
        P(("kv", "tp"), None),
    )
    out_specs = (
        P("dp", ("kv", "tp")),
        P(("dp", "kv"), "tp", None, None),
        P(("dp", "kv"), "tp", None),
        P(("dp", "kv"), "tp"),
    )
    return jax.shard_map(
        routed, mesh=mesh, in_specs=in_specs, out_specs=out_specs, check_vma=False
    )
```

time: 28.7 us -> 26.5 us (0.923)
  Pallas kernels: 27.9 us -> 25.6 us
    pallas_call x1, Pallas kernels: 26.9 us -> 24.6 us  [fused_on_device(): pl.pallas_call(functools.partial(fused_cell, n_kv, n_tp), out_shape=(jax....]
where the time goes in v1:
time: 26.5 us; the launch traced here: 26.3 us
  Pallas kernels  25.6 us (97%)
  between operations  0.65 us (2%)
    pallas_call x1, Pallas kernels, fused_on_device(): pl.pallas_call(functools.partial(fused_cell, n_kv, n_tp), out_shape=(jax....  24.6 us
    pallas_call x1, Pallas kernels, fused_on_device(): pl.pallas_call(hand_over, out_shape=tuple((jax.ShapeDtypeStruct(r.shape,...  1.01 us

profile of v1, /device:TPU:0, one launch (start us, length us, event | category | flops | bytes accessed | tf_op | source)
XLA Modules:
  0.0 26.3 jit_solution(6304362956294292669)
XLA Ops:
  0.6 24.6 %fused_cell.1 = (bf16[4,512]{1,0:T(4,128)(2,1)S(1)}, f32[1,8,256,128]{3,2,1,0:T(8,128)S(1)}, f32[1,8,128]{2,1,0:T(8,128)S(1)}, f32[1,8]{1,0:T(1,128)S(1)}) custom-call(bf16[4,512]{1,0:T(4,128)(2,1)} %tok_h.1, f32[1,4096]{1,0:T(1,128)} %bitcast.8, bf16[1024,1024]{1,0:T(8,128)(2,1)} %wq_h.1, bf16[1024,1024]{1,0:T(8,128)(2,1)} %wk_h.1, ...), custom_call_target="tpu_custom_call" | custom-call | tf_op jit(solution)/shard_map/fused_cell/pallas_call | solution.py:575
  25.3 1.0 %hand_over.1 = (bf16[4,512]{1,0:T(4,128)(2,1)}, f32[1,8,256,128]{3,2,1,0:T(8,128)}, f32[1,8,128]{2,1,0:T(8,128)}, f32[1,8]{1,0:T(1,128)}) custom-call(bf16[4,512]{1,0:T(4,128)(2,1)S(1)} %get-tuple-element.8.a, f32[1,8,256,128]{3,2,1,0:T(8,128)S(1)} %get-tuple-element.9.b, f32[1,8,128]{2,1,0:T(8,128)S(1)} %get-tuple-element.10.c, f32[1,8]{1,0:T(1,128)S(1)} %get-tuple-element.11.d), custom_call_target="tpu_custom_call" | custom-call | tf_op jit(solution)/shard_map/hand_over/pallas_call | solution.py:591

commit v2 on v1

--- a/solution.py
+++ b/solution.py
@@ -140,7 +140,7 @@
     otok, newmem, onrm, ostb,
     tok, tokall, gains, wq, wk, wv, wg, bias,
     mem, membf, nrm, stb, wo, wup, wdn,
-    own_part, part, snd, rcv, gsnd, grcv, vrow, cell_own, cell_all, y_own, y_all, mid, stage, land,
+    own_part, part, rcv, gsnd, grcv, v_own, v_snd, v_all, v_rows, v_head, cell_own, cell_all, y_own, y_all, mid, stage, land,
     load_sem, sent_sem, tok_r, rs_r, cell_r, y_r, dn_r,
 ):
     dp = lax.axis_index("dp")
@@ -156,11 +156,6 @@
     gate_count = wg.shape[0] // 2
     block = heads * LANES
     hidden = wup.shape[1]
-    TOK_S, RS_S, GATE_S, CELL_S, Y_S, DN_S = range(6)
-
-    def peer_of(offset):
-        other = (g + offset) % n_all
-        return dp, other // n_tp, other % n_tp
 
     own_span = pl.ds(pl.multiple_of(kv * span, span), span)
 
@@ -176,7 +171,7 @@
             return 3 * far_side + (1 - 2 * far_side) * step
         return (kv + i) % n_kv
 
-    chips = [chip(i) for i in range(n_kv)]
+    chips = [kv] + [chip(i) for i in range(1, n_kv)]
     far_first = chips[:0:-1]
 
     def up_rows(j):
@@ -201,8 +196,11 @@
     for c in load[:4]:
         c.start()
     barrier = pltpu.get_barrier_semaphore()
-    for o in reversed(range(1, n_all)):
-        pl.semaphore_signal(barrier, inc=1, device_id=peer_of(o), device_id_type=MESH)
+    for to in far_first:
+        for t in range(n_tp):
+            pl.semaphore_signal(barrier, inc=1, device_id=(dp, to, t), device_id_type=MESH)
+    for t in range(1, n_tp):
+        pl.semaphore_signal(barrier, inc=1, device_id=(dp, kv, (tp + t) % n_tp), device_id_type=MESH)
     for c in load[4:]:
         c.start()
 
@@ -212,7 +210,7 @@
 
     def tok_copy(to, to_tp, n):
         return pltpu.make_async_remote_copy(
-            src_ref=tok, dst_ref=tokall.at[g], send_sem=sent_sem.at[TOK_S], recv_sem=tok_r.at[n],
+            src_ref=tok, dst_ref=tokall.at[g], send_sem=sent_sem.at[0], recv_sem=tok_r.at[n],
             device_id=(dp, to, to_tp), device_id_type=MESH)
 
     for t in range(1, n_tp):
@@ -225,88 +223,76 @@
     def chunk(t):
         cols = pl.ds(pl.multiple_of((kv * n_tp + t) * thin, thin), thin)
         raw = tokall[kv * n_tp + t].astype(F32)
-        return (raw * gains[0, :, cols]).astype(BF16), jnp.sum(raw * raw, axis=1, keepdims=True)
-
-    def product(x, t, w, cols):
+        scaled = raw * gains[0, :, cols]
+        high = scaled.astype(BF16).astype(F32)
+        both = jnp.concatenate([high, scaled - high], axis=0).astype(BF16)
+        return both, jnp.sum(raw * raw, axis=1, keepdims=True)
+
+    def folded(total):
+        return total[:batch] + total[batch:]
+
+    def product(x, t, w):
         rows = pl.ds(pl.multiple_of(t * thin, thin), thin)
-        return jnp.dot(x, w[rows, cols], preferred_element_type=F32)
-
-    last = (((1,), (1,)), ((), ()))
-
-    def gate_part(x, t):
-        rows = pl.ds(pl.multiple_of(t * thin, thin), thin)
-        return lax.dot_general(x, wg[:, rows], last, preferred_element_type=F32)
-
-    whole = pl.ds(0, block)
-    columns_of = [(wq, whole, WQ), (wk, whole, WK)] + [(wv, v_cols(p), WV + p) for p in range(halves)]
-    early = 3
+        return jnp.dot(x, w[rows, :], preferred_element_type=F32)
+
     landed(gains, load_sem.at[GAINS])
-    x_own, squares = chunk(tp)
-    pending = None
-    for n, (w, cols, sem) in enumerate(columns_of[:early]):
-        landed(w.at[:, cols], load_sem.at[sem])
-        made = product(x_own, tp, w, cols)
-        if pending is not None:
-            own_part[n - 1] = pending
-        pending = made
+    x_own, _ = chunk(tp)
+    landed(wq, load_sem.at[WQ])
+    own_part[0] = product(x_own, tp, wq)
+    landed(wk, load_sem.at[WK])
+    own_part[1] = product(x_own, tp, wk)
     landed(wg, load_sem.at[WG])
-    gates_own = gate_part(x_own, tp)
-    own_part[early - 1] = pending
-    gsnd[:, 0, : 2 * gate_count] = gates_own
     landed(tokall.at[pl.ds(0, n_tp - 1)], tok_r.at[0])
-    others = [((tp + t) % n_tp, chunk((tp + t) % n_tp)) for t in range(1, n_tp)]
-    for _, (_, more) in others:
+    chunks = [chunk(t) for t in range(n_tp)]
+    x = jnp.concatenate([c for c, _ in chunks], axis=1)
+    squares = chunks[0][1]
+    for _, more in chunks[1:]:
         squares = squares + more
+
+    def mate_part(w):
+        total = None
+        for t in range(1, n_tp):
+            made = product(chunk((tp + t) % n_tp)[0], (tp + t) % n_tp, w)
+            total = made if total is None else total + made
+        return total
 
     def rs_copy(to, p):
         return pltpu.make_async_remote_copy(
-            src_ref=snd.at[to, p], dst_ref=rcv.at[kv, p],
-            send_sem=sent_sem.at[RS_S], recv_sem=rs_r.at[min(p, 2)],
+            src_ref=part.at[to, pl.ds(p * heads, heads)], dst_ref=rcv.at[kv, pl.ds(p * heads, heads)],
+            send_sem=sent_sem.at[0], recv_sem=rs_r.at[p],
             device_id=(dp, to, tp), device_id_type=MESH)
 
     def gate_copy(to):
         return pltpu.make_async_remote_copy(
             src_ref=gsnd.at[to], dst_ref=grcv.at[kv],
-            send_sem=sent_sem.at[GATE_S], recv_sem=rs_r.at[3],
+            send_sem=sent_sem.at[0], recv_sem=rs_r.at[3],
             device_id=(dp, to, tp), device_id_type=MESH)
 
     def send_part(p, total):
         for h in range(heads):
             part[:, p * heads + h, :] = total[:, h * LANES : (h + 1) * LANES]
-        for to in range(n_kv):
-            snd[to, p] = part[to, p * heads : (p + 1) * heads, :].astype(BF16)
         for to in far_first:
             rs_copy(to, p).start()
 
-    def mate_sum(of):
-        total = None
-        for t, (x_t, _) in others:
-            made = of(x_t, t)
-            total = made if total is None else total + made
-        return total
-
-    def mate_part(p):
-        w, cols, _ = columns_of[p]
-        return mate_sum(lambda x_t, t: product(x_t, t, w, cols))
-
-    pending = mate_part(0)
-    for p in range(1, len(columns_of)):
-        w, cols, sem = columns_of[p]
-        if p < early:
-            made = mate_part(p)
-        else:
-            landed(w.at[:, cols], load_sem.at[sem])
-            made = product(x_own, tp, w, cols)
-        if p == early - 1:
-            gates_mate = mate_sum(gate_part)
-        send_part(p - 1, pending + own_part[p - 1])
-        if p == early - 1:
-            gsnd[:, 0, : 2 * gate_count] = gsnd[:, 0, : 2 * gate_count] + gates_mate
-            gsnd[:, 1, :] = jnp.broadcast_to(squares, (n_kv, LANES))
-            for to in far_first:
-                gate_copy(to).start()
-        pending = made if p < early else made + mate_part(p)
-    send_part(len(columns_of) - 1, pending)
+    gates = lax.dot_general(x, wg[...], (((1,), (1,)), ((), ())), preferred_element_type=F32)
+    q_mate = mate_part(wq)
+    k_mate = mate_part(wk)
+    gsnd[:, 0, : 2 * gate_count] = folded(gates)
+    gsnd[:, 1, :] = jnp.broadcast_to(squares, (n_kv, LANES))
+    for to in far_first:
+        gate_copy(to).start()
+    send_part(0, folded(q_mate + own_part[0]))
+    send_part(1, folded(k_mate + own_part[1]))
+    for p in range(halves):
+        landed(wv.at[:, v_cols(p)], load_sem.at[WV + p])
+        made = folded(jnp.dot(x, wv[:, v_cols(p)], preferred_element_type=F32))
+        v_own[p] = made
+        v_snd[p] = made.astype(BF16)
+        for to in far_first:
+            pltpu.make_async_remote_copy(
+                src_ref=v_snd.at[p], dst_ref=v_all.at[kv, p],
+                send_sem=sent_sem.at[0], recv_sem=rs_r.at[2],
+                device_id=(dp, to, tp), device_id_type=MESH).start()
 
     landed(bias, load_sem.at[BIAS])
     landed(nrm, load_sem.at[NRM])
@@ -328,7 +314,7 @@
     def joined(p):
         total = part[kv, p * heads : (p + 1) * heads, :]
         for o in peers:
-            total = total + rcv[o, p].astype(F32)
+            total = total + rcv[o, p * heads : (p + 1) * heads, :]
         return total
 
     landed(grcv.at[pl.ds(0, n_kv - 1)], rs_r.at[3])
@@ -339,7 +325,7 @@
     gate_row = gate_sum[0:1] * scale
     gate_i = column(gate_row, 0) + column(bias[0], 0)
     gate_f = column(gate_row, gate_count) + column(bias[1], 0)
-    landed(rcv.at[pl.ds(0, n_kv - 1), 0], rs_r.at[0])
+    landed(rcv.at[pl.ds(0, n_kv - 1), pl.ds(0, heads)], rs_r.at[0])
     q = joined(0) * scale * dqk**-0.5
     log_forget = jnp.minimum(gate_f, 0.0) - jnp.log1p(jnp.exp(-jnp.abs(gate_f)))
     stab_wide = jnp.broadcast_to(stb[...], (heads, heads))
@@ -362,26 +348,29 @@
     recall = jnp.zeros((heads, dv), F32)
     for h in range(heads):
         recall = jnp.where(row_id == h, wide_recall[:, h * dv : (h + 1) * dv], recall)
-    landed(rcv.at[pl.ds(0, n_kv - 1), 1], rs_r.at[1])
+    landed(rcv.at[pl.ds(0, n_kv - 1), pl.ds(heads, heads)], rs_r.at[1])
     k = joined(1) * scale
     match = jnp.sum(q * k, axis=1, keepdims=True)
     denominator = keep * norm_dot + fresh * match
     floor_value = jnp.maximum(jnp.abs(denominator), jnp.exp(-new_stab))
-    landed(rcv.at[pl.ds(0, n_kv - 1), pl.ds(2, halves)], rs_r.at[2])
-    for p in range(halves):
-        vrow[p * heads : (p + 1) * heads, :] = joined(2 + p) * scale
-    v = jnp.concatenate([vrow[pl.ds(s, heads, stride=halves), :] for s in range(halves)], axis=1)
-    cell = (keep * recall + (fresh * match) * v) / floor_value
-    cell = cell.astype(BF16)
-    cell_own[...] = cell
-
+    cell_own[:, :dv] = keep * recall / floor_value
+    cell_own[:, dv:] = (fresh * match / floor_value) * scale
     for to in far_first:
         pltpu.make_async_remote_copy(
-            src_ref=cell_own, dst_ref=cell_all.at[kv], send_sem=sent_sem.at[CELL_S], recv_sem=cell_r.at[0],
+            src_ref=cell_own, dst_ref=cell_all.at[kv], send_sem=sent_sem.at[0], recv_sem=cell_r.at[0],
             device_id=(dp, to, tp), device_id_type=MESH).start()
-    cell_all[kv] = cell
+    cell_all[kv] = cell_own[...]
     onrm[0] = keep * nrm[...] + fresh * k
-    fresh_v = fresh * v
+    landed(v_all.at[pl.ds(0, n_kv - 1)], rs_r.at[2])
+    for p in range(halves):
+        v_sum = v_own[p]
+        for o in peers:
+            v_sum = v_sum + v_all[o, p].astype(F32)
+        v_rows[:, v_cols(p)] = v_sum
+    own_row = v_rows[pl.ds(kv, 1), :]
+    for h in range(heads):
+        v_head[h : h + 1, :] = own_row[:, h * dv : (h + 1) * dv]
+    fresh_v = (fresh * scale[:, :1]) * v_head[...]
     fresh_vt = fresh_v.T
     for h in range(heads):
         newmem[0, h] = keep[h : h + 1] * mem[h] + fresh_vt[:, h : h + 1] * k[h : h + 1]
@@ -389,8 +378,14 @@
     landed(wup, load_sem.at[WUP])
     landed(tokall.at[pl.ds(0, n_all - n_tp)], tok_r.at[1])
     landed(cell_all.at[pl.ds(0, n_kv - 1)], cell_r.at[0])
-    cells = cell_all[...].astype(F32)
-    rows = jnp.concatenate([cells[:, h, :] for h in range(heads)], axis=1).astype(BF16)
+    rows = []
+    for h in range(heads):
+        weight = cell_all[:, h, dv:]
+        for s in range(halves):
+            at = h * dv + s * LANES
+            row = cell_all[:, h, s * LANES : (s + 1) * LANES] + weight * v_rows[:, at : at + LANES]
+            rows.append(row.astype(BF16))
+    rows = jnp.concatenate(rows, axis=1)
 
     def lagged(jobs):
         pending = None
@@ -401,18 +396,21 @@
             pending = made, finish
         pending[1](pending[0])
 
+    def y_copy(c, to, t):
+        span_of = slice(None) if c is None else c
+        return pltpu.make_async_remote_copy(
+            src_ref=y_own.at[span_of], dst_ref=y_all.at[g, span_of],
+            send_sem=sent_sem.at[0], recv_sem=y_r.at[kv],
+            device_id=(dp, to, t), device_id_type=MESH)
+
     def send_y(c):
         def finish(total):
             y = total.astype(BF16)
             y_own[c] = y
-            for to in far_first + [kv]:
-                for t in range(n_tp):
-                    if t or to is not kv:
-                        to_tp = (tp + t) % n_tp
-                        pltpu.make_async_remote_copy(
-                            src_ref=y_own.at[c], dst_ref=y_all.at[g, c],
-                            send_sem=sent_sem.at[Y_S], recv_sem=y_r.at[kv, c],
-                            device_id=(dp, to, to_tp), device_id_type=MESH).start()
+            for t in range(n_tp):
+                y_copy(c, chips[1], t).start()
+            for t in range(1, n_tp):
+                y_copy(c, kv, (tp + t) % n_tp).start()
             y_all[g, c] = y
 
         return finish
@@ -422,6 +420,9 @@
         return lambda: jnp.dot(rows, wo[:, cols], preferred_element_type=F32), send_y(c)
 
     lagged([y_job(c) for c in range(n_tp)])
+    for to in chips[2:]:
+        for t in range(n_tp):
+            y_copy(None, to, t).start()
 
     square_sum = jnp.zeros((batch, 1), F32)
     total_up = [None, None]
@@ -429,11 +430,10 @@
     for i, j in enumerate(chips):
         if i == n_kv - 1:
             landed(wdn, load_sem.at[WDN])
+        landed(y_all.at[pl.ds(0, n_tp if i > 0 else n_tp - 1)], y_r.at[j])
         for wanted in ([list(range(n_tp))] if i < n_kv - 1 else [[c] for c in range(n_tp)]):
             mixed = []
             for c in wanted:
-                count = n_tp if i > 0 else n_tp - 1
-                landed(y_all.at[pl.ds(0, count), c], y_r.at[j, c])
                 base = tokall[j * n_tp + c].astype(F32)
                 for t in range(n_tp):
                     base = base + y_all[j * n_tp + t, c].astype(F32)
@@ -456,14 +456,15 @@
         up = jnp.maximum(total * scale2, 0.0)
         return (up * up).astype(BF16)
 
-    targets = [chips[i] * n_tp + (tp + t) % n_tp for i in reversed(range(n_kv)) for t in reversed(range(n_tp))]
+    targets = [to * n_tp + t for to in far_first for t in range(n_tp)]
+    targets += [kv * n_tp + (tp + t) % n_tp for t in reversed(range(n_tp))]
 
     def send_down(to):
         def finish(total):
             stage[to] = total.astype(BF16)
             pltpu.make_async_remote_copy(
                 src_ref=stage.at[to], dst_ref=land.at[g],
-                send_sem=sent_sem.at[DN_S], recv_sem=dn_r.at[0],
+                send_sem=sent_sem.at[0], recv_sem=dn_r.at[0],
                 device_id=(dp, to // n_tp, to % n_tp), device_id_type=MESH).start()
 
         return finish
@@ -479,19 +480,19 @@
 
         return make, send_down(to) if n < len(targets) - 1 else own_down.append
 
-    lagged([down_job(n, to) for n, to in enumerate(targets)])
+    down_jobs = [down_job(n, to) for n, to in enumerate(targets)]
+    down_jobs[0][1](down_jobs[0][0]())
+    lagged(down_jobs[1:])
     total = own_down[0] + mid[tp]
 
-    landed(tokall.at[pl.ds(0, n_all - 1)], sent_sem.at[TOK_S])
-    landed(snd.at[pl.ds(0, n_kv - 1)], sent_sem.at[RS_S])
-    landed(gsnd.at[pl.ds(0, n_kv - 1)], sent_sem.at[GATE_S])
-    landed(cell_all.at[pl.ds(0, n_kv - 1)], sent_sem.at[CELL_S])
-    landed(y_all.at[pl.ds(0, n_all - 1)], sent_sem.at[Y_S])
     landed(land.at[pl.ds(0, n_all - 1)], dn_r.at[0])
     for o in range(1, n_all):
         total = total + land[(g + o) % n_all].astype(F32)
     otok[...] = total.astype(BF16)
-    landed(stage.at[pl.ds(0, n_all - 1)], sent_sem.at[DN_S])
+    wide = (n_all - 1) * batch * (thin + span + thin) + (n_kv - 1) * halves * batch * block
+    narrow = (n_kv - 1) * (2 * LANES + 2 * block + heads * (dv + LANES))
+    sent = (wide + 2 * narrow) // dqk
+    landed(membf.at[pl.ds(0, sent)], sent_sem.at[0])
 
 
 def hand_over(a, b, c, d, out_a, out_b, out_c, out_d, sems):
@@ -549,22 +550,25 @@
         vm(w_output.shape, BF16),
         vm(w_up.shape, BF16),
         vm(w_down.shape, BF16),
-        vm((3, batch, heads * LANES), F32),
-        vm((n_kv, (2 + halves) * heads, LANES), F32),
-        vm((n_kv, 2 + halves, heads, LANES), BF16),
-        vm((n_kv, 2 + halves, heads, LANES), BF16),
+        vm((2, 2 * batch, heads * LANES), F32),
+        vm((n_kv, 2 * heads, LANES), F32),
+        vm((n_kv, 2 * heads, LANES), F32),
         vm((n_kv, 2, LANES), F32),
         vm((n_kv, 2, LANES), F32),
-        vm((halves * heads, LANES), F32),
-        vm((heads, dv), BF16),
-        vm((n_kv, heads, dv), BF16),
+        vm((halves, batch, heads * LANES), F32),
+        vm((halves, batch, heads * LANES), BF16),
+        vm((n_kv, halves, batch, heads * LANES), BF16),
+        vm((batch, heads * dv), F32),
+        vm((heads, dv), F32),
+        vm((heads, dv + LANES), F32),
+        vm((n_kv, heads, dv + LANES), F32),
         vm((n_tp, batch, thin), BF16),
         vm((n_all, n_tp, batch, thin), BF16),
         vm((n_tp, batch, thin), F32),
         vm((n_all, batch, thin), BF16),
         vm((n_all, batch, thin), BF16),
-        dma((12 + halves,)), dma((6,)),
-        dma((2,)), dma((4,)), dma((1,)), dma((n_kv, n_tp)), dma((1,)),
+        dma((12 + halves,)), dma((1,)),
+        dma((2,)), dma((4,)), dma((1,)), dma((n_kv,)), dma((1,)),
     ]
     args = (
         tokens, mix_gain.reshape(1, -1), w_query, w_key, w_value, w_igate.T, w_fgate.T,

time: 26.5 us -> 24.7 us (0.932)
  Pallas kernels: 25.6 us -> 23.9 us
    pallas_call x1, Pallas kernels: 24.6 us -> 22.9 us  [fused_on_device(): pl.pallas_call(functools.partial(fused_cell, n_kv, n_tp), out_shape=(jax....]
where the time goes in v2:
time: 24.7 us; the launch traced here: 24.5 us
  Pallas kernels  23.9 us (97%)
  between operations  0.65 us (3%)
    pallas_call x1, Pallas kernels, fused_on_device(): pl.pallas_call(functools.partial(fused_cell, n_kv, n_tp), out_shape=(jax....  22.9 us
    pallas_call x1, Pallas kernels, fused_on_device(): pl.pallas_call(hand_over, out_shape=tuple((jax.ShapeDtypeStruct(r.shape,...  1.01 us

profile of v2, /device:TPU:0, one launch (start us, length us, event | category | flops | bytes accessed | tf_op | source)
XLA Modules:
  0.0 24.5 jit_solution(13485636809494552434)
XLA Ops:
  0.6 22.9 %fused_cell.1 = (bf16[4,512]{1,0:T(4,128)(2,1)S(1)}, f32[1,8,256,128]{3,2,1,0:T(8,128)S(1)}, f32[1,8,128]{2,1,0:T(8,128)S(1)}, f32[1,8]{1,0:T(1,128)S(1)}) custom-call(bf16[4,512]{1,0:T(4,128)(2,1)} %tok_h.1, f32[1,4096]{1,0:T(1,128)} %bitcast.8, bf16[1024,1024]{1,0:T(8,128)(2,1)} %wq_h.1, bf16[1024,1024]{1,0:T(8,128)(2,1)} %wk_h.1, ...), custom_call_target="tpu_custom_call" | custom-call | tf_op jit(solution)/shard_map/fused_cell/pallas_call | solution.py:579
  23.5 1.0 %hand_over.1 = (bf16[4,512]{1,0:T(4,128)(2,1)}, f32[1,8,256,128]{3,2,1,0:T(8,128)}, f32[1,8,128]{2,1,0:T(8,128)}, f32[1,8]{1,0:T(1,128)}) custom-call(bf16[4,512]{1,0:T(4,128)(2,1)S(1)} %get-tuple-element.8.a, f32[1,8,256,128]{3,2,1,0:T(8,128)S(1)} %get-tuple-element.9.b, f32[1,8,128]{2,1,0:T(8,128)S(1)} %get-tuple-element.10.c, f32[1,8]{1,0:T(1,128)S(1)} %get-tuple-element.11.d), custom_call_target="tpu_custom_call" | custom-call | tf_op jit(solution)/shard_map/hand_over/pallas_call | solution.py:595

commit v3 on v2

--- a/solution.py
+++ b/solution.py
@@ -140,8 +140,8 @@
     otok, newmem, onrm, ostb,
     tok, tokall, gains, wq, wk, wv, wg, bias,
     mem, membf, nrm, stb, wo, wup, wdn,
-    own_part, part, rcv, gsnd, grcv, v_own, v_snd, v_all, v_rows, v_head, cell_own, cell_all, y_own, y_all, mid, stage, land,
-    load_sem, sent_sem, tok_r, rs_r, cell_r, y_r, dn_r,
+    part, rcv, gsnd, grcv, v_own, v_snd, v_all, v_rows, v_head, cell_own, cell_all, y_own, y_all, mid, stage, land,
+    load_sem, sent_sem, tok_r, rs_r, cell_r, y_r, dn_r, pair_sem,
 ):
     dp = lax.axis_index("dp")
     kv = lax.axis_index("kv")
@@ -173,16 +173,22 @@
 
     chips = [kv] + [chip(i) for i in range(1, n_kv)]
     far_first = chips[:0:-1]
+    down_first, y_first = far_first, chips[1:]
+    if n_kv == 4:
+        low = near * (1 - far_side)
+        swap = low * (far_first[1] - far_first[0])
+        down_first = [far_first[0] + swap, far_first[1] - swap, far_first[2]]
+        y_first = [near * a + (1 - near) * b for a, b in zip(chips[1:], far_first)]
 
     def up_rows(j):
         return pl.ds(pl.multiple_of(j * span, span), span)
 
-    TOK, GAINS, WQ, WK, WG, BIAS, NRM, STB, MEM, WO, WUP, WDN, WV = range(13)
+    TOK, GAINS, WQ, WK, WG, BIAS, NRM, STB, MEM, WO, WUP, WDN, WDN_REST, WV = range(14)
     loads = [
         (tok_h, tok, TOK), (mixg_h, gains.at[0], GAINS), (mlpg_h, gains.at[1], GAINS), (wq_h, wq, WQ),
-        (wk_h, wk, WK),
         (wig_h.at[:, own_span], wg.at[pl.ds(0, gate_count)], WG),
         (wfg_h.at[:, own_span], wg.at[pl.ds(gate_count, gate_count)], WG),
+        (wk_h, wk, WK),
     ]
     loads += [(wv_h.at[:, v_cols(p)], wv.at[:, v_cols(p)], WV + p) for p in range(halves)]
     loads += [
@@ -190,23 +196,36 @@
         (mem_h.at[0], mem, MEM), (wo_h, wo, WO),
     ]
     loads += [(wup_h.at[up_rows(j)], wup.at[up_rows(j)], WUP) for j in chips]
-    loads += [(wdn_h, wdn, WDN)]
+    for n, to in enumerate(down_first + [kv]):
+        loads += [(wdn_h.at[:, up_rows(to)], wdn.at[:, up_rows(to)], WDN_REST if n else WDN)]
     load = [pltpu.make_async_copy(x, y, load_sem.at[n]) for x, y, n in loads]
 
-    for c in load[:4]:
+    barrier = pltpu.get_barrier_semaphore()
+    mate = (dp, kv, 1 - tp)
+
+    def signal(sem, to):
+        pl.semaphore_signal(sem, inc=1, device_id=to, device_id_type=MESH)
+
+    @pl.when(tp == 0)
+    def _():
+        signal(barrier, mate)
+
+    for c in load:
         c.start()
-    barrier = pltpu.get_barrier_semaphore()
-    for to in far_first:
-        for t in range(n_tp):
-            pl.semaphore_signal(barrier, inc=1, device_id=(dp, to, t), device_id_type=MESH)
-    for t in range(1, n_tp):
-        pl.semaphore_signal(barrier, inc=1, device_id=(dp, kv, (tp + t) % n_tp), device_id_type=MESH)
-    for c in load[4:]:
-        c.start()
+
+    @pl.when(tp == 1)
+    def _():
+        pl.semaphore_wait(barrier, 1)
+        signal(pair_sem, mate)
+
+    @pl.when(tp == 0)
+    def _():
+        pl.semaphore_wait(pair_sem, 1)
+        for to in far_first:
+            signal(barrier, (dp, to, 0))
 
     gsnd[...] = jnp.zeros(gsnd.shape, F32)
     landed(tok, load_sem.at[TOK])
-    pl.semaphore_wait(barrier, n_all - 1)
 
     def tok_copy(to, to_tp, n):
         return pltpu.make_async_remote_copy(
@@ -216,9 +235,6 @@
     for t in range(1, n_tp):
         tok_copy(kv, (tp + t) % n_tp, 0).start()
     tokall[g] = tok[...]
-    for to in far_first:
-        for t in range(n_tp):
-            tok_copy(to, (tp + t) % n_tp, 1).start()
 
     def chunk(t):
         cols = pl.ds(pl.multiple_of((kv * n_tp + t) * thin, thin), thin)
@@ -231,17 +247,7 @@
     def folded(total):
         return total[:batch] + total[batch:]
 
-    def product(x, t, w):
-        rows = pl.ds(pl.multiple_of(t * thin, thin), thin)
-        return jnp.dot(x, w[rows, :], preferred_element_type=F32)
-
     landed(gains, load_sem.at[GAINS])
-    x_own, _ = chunk(tp)
-    landed(wq, load_sem.at[WQ])
-    own_part[0] = product(x_own, tp, wq)
-    landed(wk, load_sem.at[WK])
-    own_part[1] = product(x_own, tp, wk)
-    landed(wg, load_sem.at[WG])
     landed(tokall.at[pl.ds(0, n_tp - 1)], tok_r.at[0])
     chunks = [chunk(t) for t in range(n_tp)]
     x = jnp.concatenate([c for c, _ in chunks], axis=1)
@@ -249,13 +255,6 @@
     for _, more in chunks[1:]:
         squares = squares + more
 
-    def mate_part(w):
-        total = None
-        for t in range(1, n_tp):
-            made = product(chunk((tp + t) % n_tp)[0], (tp + t) % n_tp, w)
-            total = made if total is None else total + made
-        return total
-
     def rs_copy(to, p):
         return pltpu.make_async_remote_copy(
             src_ref=part.at[to, pl.ds(p * heads, heads)], dst_ref=rcv.at[kv, pl.ds(p * heads, heads)],
@@ -268,21 +267,49 @@
             send_sem=sent_sem.at[0], recv_sem=rs_r.at[3],
             device_id=(dp, to, tp), device_id_type=MESH)
 
-    def send_part(p, total):
+    def keep_part(p, total):
         for h in range(heads):
             part[:, p * heads + h, :] = total[:, h * LANES : (h + 1) * LANES]
+
+    def first_sends():
+        @pl.when(tp == 0)
+        def _():
+            pl.semaphore_wait(barrier, n_kv - 1)
+            signal(pair_sem, mate)
+
+        @pl.when(tp == 1)
+        def _():
+            pl.semaphore_wait(pair_sem, 1)
+
         for to in far_first:
-            rs_copy(to, p).start()
-
+            gate_copy(to).start()
+        for to in far_first:
+            rs_copy(to, 0).start()
+
+    landed(wq, load_sem.at[WQ])
+    q_all = jnp.dot(x, wq[...], preferred_element_type=F32)
+    landed(wg, load_sem.at[WG])
     gates = lax.dot_general(x, wg[...], (((1,), (1,)), ((), ())), preferred_element_type=F32)
-    q_mate = mate_part(wq)
-    k_mate = mate_part(wk)
     gsnd[:, 0, : 2 * gate_count] = folded(gates)
     gsnd[:, 1, :] = jnp.broadcast_to(squares, (n_kv, LANES))
+    keep_part(0, folded(q_all))
+
+    @pl.when(2 * kv >= n_kv)
+    def _():
+        first_sends()
+
+    landed(wk, load_sem.at[WK])
+    keep_part(1, folded(jnp.dot(x, wk[...], preferred_element_type=F32)))
+
+    @pl.when(2 * kv < n_kv)
+    def _():
+        first_sends()
+
     for to in far_first:
-        gate_copy(to).start()
-    send_part(0, folded(q_mate + own_part[0]))
-    send_part(1, folded(k_mate + own_part[1]))
+        rs_copy(to, 1).start()
+    for to in far_first:
+        for t in range(n_tp):
+            tok_copy(to, (tp + t) % n_tp, 1).start()
     for p in range(halves):
         landed(wv.at[:, v_cols(p)], load_sem.at[WV + p])
         made = folded(jnp.dot(x, wv[:, v_cols(p)], preferred_element_type=F32))
@@ -375,7 +402,6 @@
     for h in range(heads):
         newmem[0, h] = keep[h : h + 1] * mem[h] + fresh_vt[:, h : h + 1] * k[h : h + 1]
     landed(wo, load_sem.at[WO])
-    landed(wup, load_sem.at[WUP])
     landed(tokall.at[pl.ds(0, n_all - n_tp)], tok_r.at[1])
     landed(cell_all.at[pl.ds(0, n_kv - 1)], cell_r.at[0])
     rows = []
@@ -396,21 +422,16 @@
             pending = made, finish
         pending[1](pending[0])
 
-    def y_copy(c, to, t):
-        span_of = slice(None) if c is None else c
-        return pltpu.make_async_remote_copy(
-            src_ref=y_own.at[span_of], dst_ref=y_all.at[g, span_of],
-            send_sem=sent_sem.at[0], recv_sem=y_r.at[kv],
-            device_id=(dp, to, t), device_id_type=MESH)
-
     def send_y(c):
         def finish(total):
             y = total.astype(BF16)
             y_own[c] = y
-            for t in range(n_tp):
-                y_copy(c, chips[1], t).start()
-            for t in range(1, n_tp):
-                y_copy(c, kv, (tp + t) % n_tp).start()
+            for to in y_first[:1] + [kv] + y_first[1:]:
+                for t in range(1 if to is kv else 0, n_tp):
+                    pltpu.make_async_remote_copy(
+                        src_ref=y_own.at[c], dst_ref=y_all.at[g, c],
+                        send_sem=sent_sem.at[0], recv_sem=y_r.at[kv, c],
+                        device_id=(dp, to, (tp + t) % n_tp if to is kv else t), device_id_type=MESH).start()
             y_all[g, c] = y
 
         return finish
@@ -420,18 +441,18 @@
         return lambda: jnp.dot(rows, wo[:, cols], preferred_element_type=F32), send_y(c)
 
     lagged([y_job(c) for c in range(n_tp)])
-    for to in chips[2:]:
-        for t in range(n_tp):
-            y_copy(None, to, t).start()
-
+
+    landed(wup, load_sem.at[WUP])
     square_sum = jnp.zeros((batch, 1), F32)
     total_up = [None, None]
     cut = hidden // 2
     for i, j in enumerate(chips):
         if i == n_kv - 1:
-            landed(wdn, load_sem.at[WDN])
-        landed(y_all.at[pl.ds(0, n_tp if i > 0 else n_tp - 1)], y_r.at[j])
-        for wanted in ([list(range(n_tp))] if i < n_kv - 1 else [[c] for c in range(n_tp)]):
+            landed(wdn.at[:, pl.ds(0, span)], load_sem.at[WDN])
+        whole = i == 0 or 1 < i < n_kv - 1
+        for wanted in ([list(range(n_tp))] if whole else [[c] for c in range(n_tp)]):
+            for c in wanted:
+                landed(y_all.at[pl.ds(0, n_tp if i > 0 else n_tp - 1), c], y_r.at[j, c])
             mixed = []
             for c in wanted:
                 base = tokall[j * n_tp + c].astype(F32)
@@ -456,7 +477,7 @@
         up = jnp.maximum(total * scale2, 0.0)
         return (up * up).astype(BF16)
 
-    targets = [to * n_tp + t for to in far_first for t in range(n_tp)]
+    targets = [to * n_tp + t for to in down_first for t in range(n_tp)]
     targets += [kv * n_tp + (tp + t) % n_tp for t in reversed(range(n_tp))]
 
     def send_down(to):
@@ -482,6 +503,7 @@
 
     down_jobs = [down_job(n, to) for n, to in enumerate(targets)]
     down_jobs[0][1](down_jobs[0][0]())
+    landed(wdn.at[:, pl.ds(0, (n_kv - 1) * span)], load_sem.at[WDN_REST])
     lagged(down_jobs[1:])
     total = own_down[0] + mid[tp]
 
@@ -513,7 +535,7 @@
     return (
         own_rows == 1 and batch == n_kv and heads == 8 and dqk == LANES and dv % LANES == 0
         and w_query.shape[1] == heads * dqk and w_value.shape[1] == heads * dv
-        and thin % (2 * LANES) == 0 and span == n_tp * thin and n_kv >= 2 and n_tp >= 2
+        and thin % (2 * LANES) == 0 and span == n_tp * thin and n_kv >= 2 and n_tp == 2
         and w_output.shape[1] == span and held < 52 * 2**20
     )
 
@@ -550,7 +572,6 @@
         vm(w_output.shape, BF16),
         vm(w_up.shape, BF16),
         vm(w_down.shape, BF16),
-        vm((2, 2 * batch, heads * LANES), F32),
         vm((n_kv, 2 * heads, LANES), F32),
         vm((n_kv, 2 * heads, LANES), F32),
         vm((n_kv, 2, LANES), F32),
@@ -567,8 +588,9 @@
         vm((n_tp, batch, thin), F32),
         vm((n_all, batch, thin), BF16),
         vm((n_all, batch, thin), BF16),
-        dma((12 + halves,)), dma((1,)),
-        dma((2,)), dma((4,)), dma((1,)), dma((n_kv,)), dma((1,)),
+        dma((13 + halves,)), dma((1,)),
+        dma((2,)), dma((4,)), dma((1,)), dma((n_kv, n_tp)), dma((1,)),
+        pltpu.SemaphoreType.REGULAR,
     ]
     args = (
         tokens, mix_gain.reshape(1, -1), w_query, w_key, w_value, w_igate.T, w_fgate.T,

time: 24.7 us -> 24.1 us (0.976)
  Pallas kernels: 23.9 us -> 23.3 us
    pallas_call x1, Pallas kernels: 22.9 us -> 22.3 us  [fused_on_device(): pl.pallas_call(functools.partial(fused_cell, n_kv, n_tp), out_shape=(jax....]
where the time goes in v3:
time: 24.1 us; the launch traced here: 23.9 us
  Pallas kernels  23.3 us (97%)
  between operations  0.65 us (3%)
    pallas_call x1, Pallas kernels, fused_on_device(): pl.pallas_call(functools.partial(fused_cell, n_kv, n_tp), out_shape=(jax....  22.3 us
    pallas_call x1, Pallas kernels, fused_on_device(): pl.pallas_call(hand_over, out_shape=tuple((jax.ShapeDtypeStruct(r.shape,...  1.01 us

profile of v3, /device:TPU:0, one launch (start us, length us, event | category | flops | bytes accessed | tf_op | source)
XLA Modules:
  0.0 23.9 jit_solution(7208111861492675075)
XLA Ops:
  0.6 22.3 %fused_cell.1 = (bf16[4,512]{1,0:T(4,128)(2,1)S(1)}, f32[1,8,256,128]{3,2,1,0:T(8,128)S(1)}, f32[1,8,128]{2,1,0:T(8,128)S(1)}, f32[1,8]{1,0:T(1,128)S(1)}) custom-call(bf16[4,512]{1,0:T(4,128)(2,1)} %tok_h.1, f32[1,4096]{1,0:T(1,128)} %bitcast.8, bf16[1024,1024]{1,0:T(8,128)(2,1)} %wq_h.1, bf16[1024,1024]{1,0:T(8,128)(2,1)} %wk_h.1, ...), custom_call_target="tpu_custom_call" | custom-call | tf_op jit(solution)/shard_map/fused_cell/pallas_call | solution.py:601
  22.9 1.0 %hand_over.1 = (bf16[4,512]{1,0:T(4,128)(2,1)}, f32[1,8,256,128]{3,2,1,0:T(8,128)}, f32[1,8,128]{2,1,0:T(8,128)}, f32[1,8]{1,0:T(1,128)}) custom-call(bf16[4,512]{1,0:T(4,128)(2,1)S(1)} %get-tuple-element.8.a, f32[1,8,256,128]{3,2,1,0:T(8,128)S(1)} %get-tuple-element.9.b, f32[1,8,128]{2,1,0:T(8,128)S(1)} %get-tuple-element.10.c, f32[1,8]{1,0:T(1,128)S(1)} %get-tuple-element.11.d), custom_call_target="tpu_custom_call" | custom-call | tf_op jit(solution)/shard_map/hand_over/pallas_call | solution.py:617
